TPU v7x, 128 devices: a whole 4x4x4 slice. The times are simulated.
128 devices in a mesh: kv: 16 (over z, x), tp: 8 (over y, core).
Axes of the slice: x: 4, y: 4, z: 4, core: 2. Of those that a mesh axis runs over, the one named last changes fastest.
Arguments:
- tokens: bfloat16 [288, 4096], P(None, 'kv'), may hold values from -40 to 40
- norm_gain: float32 [4096], P('kv'), may hold values from 0.1 to 1.9
- query_weight: bfloat16 [4096, 2048], P('kv', 'tp'), may hold values from -0.09375 to 0.09375
- key_weight: bfloat16 [4096, 2048], P('kv', 'tp'), may hold values from -0.09375 to 0.09375
- value_weight: bfloat16 [4096, 2048], P('kv', 'tp'), may hold values from -0.09375 to 0.09375
- gate_weight: bfloat16 [4096, 32], replicated, may hold values from -0.09375 to 0.09375
- gate_bias: float32 [32], replicated, may hold values from -0.5 to 3
- out_weight: bfloat16 [2048, 4096], P('tp', 'kv'), may hold values from -0.125 to 0.125
- cache_keys: bfloat16 [12, 6144, 2048], P(None, 'kv', 'tp'), may hold values from -1000 to 1000
- cache_values: bfloat16 [12, 6144, 2048], P(None, 'kv', 'tp'), may hold values from -6 to 6
- cache_decay: float32 [12, 32, 6144], P(None, 'tp', 'kv'), may hold values from -6144 to 0, as said below
- lengths: int32 [12], replicated, may hold values from 3073 to 6144
- parents: int32 [12, 24], replicated, may hold values from 0 to 23, as said below
Outputs:
- mixed: bfloat16 [288, 4096], P('tp', 'kv')
Inputs may be any that keep to these rules, and one draw needn't show every extreme that they name: `cache_decay`: zero at and beyond lengths of the sequence. parents[s, 0] = 0 and parents[s, n] < n for n > 0.
All inputs are finite; a program needn't handle non-finite values.
Results may differ from a plain program's by a relative error of at most 0.014.
The roundings to bfloat16 on the way count: a program that leaves them out, or rounds other values in their place, can miss the bound.
Values may be sent and summed in bfloat16 or wider, within the bound.
A program may use at most 64 MiB of HBM per device.

v0:
```python
import math

import jax
import jax.numpy as jnp
from jax import lax
from jax.sharding import PartitionSpec as P


def in_blocks(x, dim, devices):
    shape = x.shape
    pieces = x.reshape(*shape[:dim], devices, shape[dim] // devices, *shape[dim + 1 :])
    return jnp.moveaxis(pieces, dim, 0)


def sum_at_owner(x, axis, dim):
    pieces = in_blocks(x, dim, lax.axis_size(axis))
    arrived = lax.all_to_all(pieces, axis, split_axis=0, concat_axis=0, tiled=True)
    return arrived.sum(axis=0)


def in_one_piece(arrays, axis, dim, along):
    columns = [a.reshape(*a.shape[:along], -1) for a in arrays]
    both = jnp.concatenate(columns, axis=along)
    filled, at, outs = (sum_at_owner(both, axis, dim), 0, [])
    for a, column in zip(arrays, columns):
        section = filled[..., at : at + column.shape[along]]
        outs.append(section.reshape(*section.shape[:along], *a.shape[along:]))
        at += column.shape[along]
    return tuple(outs)


def copy_for_each(x, axis):
    copies = jnp.broadcast_to(x, (lax.axis_size(axis), *x.shape))
    return lax.all_to_all(copies, axis, split_axis=0, concat_axis=0, tiled=True)


def laid_out(pieces, dim):
    shape = list(pieces.shape[1:])
    shape[dim] *= pieces.shape[0]
    return jnp.moveaxis(pieces, 0, dim).reshape(shape)


def gathered_copies(x, axis, dim):
    pieces = copy_for_each(x, axis)
    return laid_out(pieces, dim)


def in_one_piece_2(arrays, axis, split_dim, concat_dim, along):
    widths = [math.prod(a.shape[along:]) for a in arrays]
    both = jnp.concatenate(
        [a.reshape(*a.shape[:along], w) for a, w in zip(arrays, widths)], axis=along
    )
    filled = lax.all_to_all(both, axis, split_axis=split_dim, concat_axis=concat_dim, tiled=True)
    pieces = jnp.split(filled, [sum(widths[:k]) for k in range(1, len(widths))], axis=along)
    return tuple(
        (b.reshape(*filled.shape[:along], *a.shape[along:]) for a, b in zip(arrays, pieces))
    )


def summed_on_arrival(x, axis, dim):
    devices = lax.axis_size(axis)
    pieces = lax.all_to_all(in_blocks(x, dim, devices), axis, 0, 0, tiled=True)
    return jnp.sum(pieces.astype(jnp.float32), axis=0)


def ancestry_of(parents):
    count = parents.shape[1]
    nodes = jnp.arange(count, dtype=jnp.int32)
    link = (parents[:, :, None] == nodes[None, None, :]).astype(jnp.float32)
    link = jnp.maximum(link, jnp.eye(count, dtype=jnp.float32)[None])
    for _ in range(count.bit_length()):
        link = jnp.minimum(jnp.einsum("snm,smk->snk", link, link), 1.0)
    return link


def finish(cache_top, cache_total, cache_mix, tree_top, tree_total, tree_mix):
    top = jnp.maximum(cache_top, tree_top)
    cache_factor = jnp.exp(cache_top - top)
    tree_factor = jnp.exp(tree_top - top)
    numer = cache_factor[..., None] * cache_mix + tree_factor[..., None] * tree_mix
    denom = cache_factor * cache_total + tree_factor * tree_total
    return (numer / denom[..., None]).astype(jnp.bfloat16)


def body(
    tokens,
    norm_gain,
    query_weight,
    key_weight,
    value_weight,
    gate_weight,
    gate_bias,
    out_weight,
    cache_keys,
    cache_values,
    cache_decay,
    lengths,
    parents,
):
    rows, width_dev = tokens.shape
    seqs, props = parents.shape
    heads_dev = cache_decay.shape[1]
    pos_dev = cache_keys.shape[1]
    head_dim = query_weight.shape[1] // heads_dev
    scale = head_dim ** (-0.5)
    kv_index = lax.axis_index("kv")
    tp_index = lax.axis_index("tp")
    full_width = width_dev * lax.axis_size("kv")
    xf = tokens.astype(jnp.float32)
    squares = jnp.sum(xf * xf, axis=1)
    normed = (xf * norm_gain).astype(jnp.bfloat16)
    gate_rows = lax.dynamic_slice_in_dim(gate_weight, kv_index * width_dev, width_dev, 0)
    stacked = jnp.stack(
        [
            jnp.dot(normed, weight, preferred_element_type=jnp.float32)
            for weight in (query_weight, key_weight, value_weight)
        ],
        axis=1,
    )
    gate_part = jnp.dot(normed, gate_rows, preferred_element_type=jnp.float32)
    stacked, gate_part, squares = in_one_piece((stacked, gate_part, squares), "kv", 0, 1)
    inverse = lax.rsqrt(squares / full_width + 1e-06)[:, None]
    fresh = gathered_copies((inverse[:, :, None] * stacked).astype(jnp.bfloat16), "kv", 0)
    log_gates = gathered_copies(jax.nn.log_sigmoid(inverse * gate_part + gate_bias), "kv", 0)
    own_gates = lax.dynamic_slice_in_dim(log_gates, tp_index * heads_dev, heads_dev, 1).reshape(
        seqs, props, heads_dev
    )
    queries = fresh[:, 0].reshape(seqs, props, heads_dev, head_dim)
    new_keys = fresh[:, 1].reshape(seqs, props, heads_dev, head_dim)
    new_values = fresh[:, 2].reshape(seqs, props, heads_dev, head_dim)
    ancestry = ancestry_of(parents)
    path = jnp.einsum("snk,skh->snh", ancestry, own_gates)
    keys = cache_keys.reshape(seqs, pos_dev, heads_dev, head_dim)
    values = cache_values.reshape(seqs, pos_dev, heads_dev, head_dim)
    scores = (
        jnp.einsum("snhd,sjhd->snhj", queries, keys, preferred_element_type=jnp.float32) * scale
    )
    scores = scores + path[..., None] + cache_decay[:, None, :, :]
    position = kv_index * pos_dev + jnp.arange(pos_dev, dtype=jnp.int32)
    live = (position[None, :] < lengths[:, None])[:, None, None, :]
    scores = jnp.where(live, scores, -1e30)
    cache_top = jnp.max(scores, axis=-1)
    weights = jnp.where(live, jnp.exp(scores - cache_top[..., None]), 0.0)
    cache_total = jnp.sum(weights, axis=-1).reshape(rows, heads_dev)
    cache_mix = jnp.einsum(
        "snhj,sjhd->snhd", weights.astype(jnp.bfloat16), values, preferred_element_type=jnp.float32
    ).reshape(rows, heads_dev, head_dim)
    cache_top = cache_top.reshape(rows, heads_dev)
    tree_scores = (
        jnp.einsum("snhd,skhd->snhk", queries, new_keys, preferred_element_type=jnp.float32) * scale
    )
    tree_scores = tree_scores + path[..., None] - jnp.swapaxes(path, 1, 2)[:, None, :, :]
    tree_live = ancestry[:, :, None, :] > 0.5
    tree_scores = jnp.where(tree_live, tree_scores, -1e30)
    tree_top = jnp.max(tree_scores, axis=-1)
    tree_weights = jnp.where(tree_live, jnp.exp(tree_scores - tree_top[..., None]), 0.0)
    tree_total = jnp.sum(tree_weights, axis=-1).reshape(rows, heads_dev)
    tree_mix = jnp.einsum(
        "snhk,skhd->snhd",
        tree_weights.astype(jnp.bfloat16),
        new_values,
        preferred_element_type=jnp.float32,
    ).reshape(rows, heads_dev, head_dim)
    tree_top = tree_top.reshape(rows, heads_dev)
    block = rows // lax.axis_size("kv")
    tops, totals, mixes = in_one_piece_2(
        (cache_top[None], cache_total[None], cache_mix[None]), "kv", 1, 0, 3
    )
    best = jnp.max(tops, axis=0)
    factors = jnp.exp(tops - best[None])
    merged_total = jnp.sum(factors * totals, axis=0)
    merged_mix = jnp.sum(factors[..., None] * mixes, axis=0)
    start = kv_index * block
    piece = finish(
        best,
        merged_total,
        merged_mix,
        lax.dynamic_slice_in_dim(tree_top, start, block, 0),
        lax.dynamic_slice_in_dim(tree_total, start, block, 0),
        lax.dynamic_slice_in_dim(tree_mix, start, block, 0),
    )
    attended = gathered_copies(piece.reshape(block, heads_dev * head_dim), "kv", 0)
    term = jnp.dot(attended, out_weight, preferred_element_type=jnp.float32)
    return summed_on_arrival(term.astype(jnp.bfloat16), "tp", 0).astype(jnp.bfloat16)


def solution(mesh):
    in_specs = (
        P(None, "kv"),
        P("kv"),
        P("kv", "tp"),
        P("kv", "tp"),
        P("kv", "tp"),
        P(),
        P(),
        P("tp", "kv"),
        P(None, "kv", "tp"),
        P(None, "kv", "tp"),
        P(None, "tp", "kv"),
        P(),
        P(),
    )
    out_specs = P("tp", "kv")
    return jax.shard_map(body, mesh=mesh, in_specs=in_specs, out_specs=out_specs, check_vma=False)
```

profile of v0, /device:TPU:1, one launch (start us, length us, event | category | flops | bytes accessed | tf_op | source)
XLA Modules:
  0.0 114.5 jit_solution(5071618361405481364)
XLA Ops:
  0.0 1.1 fusion.16
  1.2 1.1 fusion.27
  2.3 0.2 concatenate.14
  2.5 0.2 copy.192
  2.7 1.2 %convolution_bitcast_fusion.2 = f32[288,1,256]{2,0,1:T(8,128)S(1)} fusion(bf16[256,256]{1,0:T(8,128)(2,1)} %param.17, bf16[288,256]{1,0:T(8,128)(2,1)} %param.13, f32[256]{0:T(256)} %param.14), kind=kOutput, calls=%fused_computation.14 | convolution fusion | flops 37969920 | bytes 574464 | tf_op jit(solution)/shard_map/dot_general | solution.py:115
  3.9 0.9 convolution_bitcast_fusion.3
  4.8 0.2 convolution_bitcast_fusion.4
  5.0 0.6 copy.191
  5.7 0.6 concatenate.13
  6.3 0.2 concatenate.18
  6.5 1.2 %pad_maximum_fusion = f32[16,18,801]{2,1,0:T(8,128)} fusion(f32[16,18,1]{2,1,0:T(8,128)S(1)} %concatenate.18, f32[16,18,32]{2,1,0:T(8,128)S(1)} %copy.192, f32[16,18,768]{2,1,0:T(8,128)S(1)} %concatenate.13), kind=kLoop, calls=%fused_computation.6 | loop fusion | flops 461376 | bytes 1845504 | tf_op jit(solution)/shard_map/concatenate | solution.py:23
  7.7 8.5 %all-to-all-start = ((f32[16,18,801]{2,1,0:T(8,128)}), f32[16,18,801]{2,1,0:T(8,128)S(1)}, u32[]{:S(2)}, u32[]{:S(2)}) async-start(f32[16,18,801]{2,1,0:T(8,128)} %pad_maximum_fusion), calls=%async_computation | async-start | bytes 2752512 | tf_op jit(solution)/shard_map/all_to_all | solution.py:17
  16.3 0.3 convolution_minimum_fusion.4
  16.6 0.4 convolution_minimum_fusion.2
  17.0 0.4 broadcast_compare_fusion
  17.3 19.0 %all-to-all-done = f32[16,18,801]{2,1,0:T(8,128)S(1)} async-done(((f32[16,18,801]{2,1,0:T(8,128)}), f32[16,18,801]{2,1,0:T(8,128)S(1)}, u32[]{:S(2)}, u32[]{:S(2)}) %all-to-all-start) | async-done | bytes 922784 | tf_op jit(solution)/shard_map/all_to_all | solution.py:17
  36.3 0.1 reduce_sum.67
  36.4 0.2 fusion.49
  36.6 0.1 fusion.44
  36.7 0.7 reshape.131
  37.4 5.1 %all-to-all-start.2 = ((bf16[16,2,288]{2,1,0:T(2,128)(2,1)}), bf16[16,2,288]{2,1,0:T(2,128)(2,1)S(1)}, u32[]{:S(2)}, u32[]{:S(2)}) async-start(bf16[16,2,288]{2,1,0:T(2,128)(2,1)} %reshape.131), calls=%async_computation.2 | async-start | bytes 49152 | tf_op jit(solution)/shard_map/all_to_all | solution.py:34
  42.6 0.1 multiply_convert_fusion
  42.7 6.3 %all-to-all-done.2 = bf16[16,2,288]{2,1,0:T(2,128)(2,1)S(1)} async-done(((bf16[16,2,288]{2,1,0:T(2,128)(2,1)}), bf16[16,2,288]{2,1,0:T(2,128)(2,1)S(1)}, u32[]{:S(2)}, u32[]{:S(2)}) %all-to-all-start.2) | async-done | bytes 18464 | tf_op jit(solution)/shard_map/all_to_all | solution.py:34
  49.0 0.9 broadcast_in_dim.67
  49.9 3.6 %all-to-all-start.1 = ((bf16[16,18,3,256]{3,1,2,0:T(8,128)(2,1)}), bf16[16,18,3,256]{3,1,2,0:T(8,128)(2,1)S(1)}, u32[]{:S(2)}, u32[]{:S(2)}) async-start(bf16[16,18,3,256]{3,1,2,0:T(8,128)(2,1)} %broadcast_in_dim.67), calls=%async_computation.1 | async-start | bytes 1179648 | tf_op jit(solution)/shard_map/all_to_all | solution.py:34
  53.5 0.1 broadcast_compare_fusion.1
  53.6 2.4 %copy.196 = bf16[12,384,256]{1,2,0:T(8,128)(2,1)} copy(bf16[12,384,256]{2,1,0:T(8,128)(2,1)S(1)} %copy-done.2) | data formatting | bytes 4718592 | tf_op args[8]
  56.0 4.3 %copy.202 = bf16[12,384,256]{1,2,0:T(8,128)(2,1)} copy(bf16[12,384,256]{2,1,0:T(8,128)(2,1)} %param.22) | data formatting | bytes 4718592 | tf_op args[9]
  60.3 0.1 copy.209
  60.4 0.1 reshape.132
  60.6 0.1 constant_dynamic-slice_fusion.1
  60.7 0.2 fusion.62
  60.9 2.9 %all-to-all-done.1 = bf16[16,18,3,256]{3,1,2,0:T(8,128)(2,1)S(1)} async-done(((bf16[16,18,3,256]{3,1,2,0:T(8,128)(2,1)}), bf16[16,18,3,256]{3,1,2,0:T(8,128)(2,1)S(1)}, u32[]{:S(2)}, u32[]{:S(2)}) %all-to-all-start.1) | async-done | bytes 442400 | tf_op jit(solution)/shard_map/all_to_all | solution.py:34
  63.8 0.1 reshape.116
  64.0 0.2 reshape_squeeze.9
  64.2 2.4 %fusion.61 = (f32[12,24,4]{1,2,0:T(4,128)S(1)}, f32[12,24,4,384]{3,1,2,0:T(8,128)S(1)}) fusion(f32[12,4,384]{2,1,0:T(4,128)S(1)} %copy-done.6, f32[12,24,4]{1,2,0:T(4,128)S(1)} %fusion.62, bf16[12,384,4,64]{1,3,2,0:T(8,128)(2,1)} %bitcast.73, bf16[12,24,4,64]{3,2,1,0:T(4,128)(2,1)S(1)} %reshape_squeeze.9, pred[12,384]{1,0:T(8,128)(4,1)S(1)} %broadcast_compare_fusion.1), kind=kOutput, calls=%fused_computation.93 | convolution fusion | flops 58833792 | bytes 4363776 | tf_op jit(solution)/shard_map/snhd,sjhd->snhj/dot_general | solution.py:136
  66.6 0.6 fusion.3
  67.3 0.2 reshape_broadcast_in_dim_reshape.9
  67.5 2.7 %convolution_bitcast_fusion.1 = f32[12,24,4,64]{3,1,2,0:T(8,128)S(1)} fusion(bf16[12,384,4,64]{1,3,2,0:T(8,128)(2,1)} %bitcast.72, f32[12,24,4,384]{3,1,2,0:T(8,128)S(1)} %get-tuple-element.19, f32[12,24,4]{1,2,0:T(4,128)S(1)} %get-tuple-element.18, pred[12,384]{1,0:T(8,128)(4,1)S(1)} %broadcast_compare_fusion.1), kind=kOutput, calls=%fused_computation.13 | convolution fusion | flops 57950208 | bytes 4432896 | tf_op jit(solution)/shard_map/snhj,sjhd->snhd/dot_general | solution.py:145
  70.2 0.2 reshape_broadcast_in_dim_reshape.8
  70.4 0.4 pad_maximum_fusion.2
  70.8 1.2 %copy.206 = f32[1,288,4,66]{3,2,0,1:T(4,128)} copy(f32[1,288,4,66]{3,1,2,0:T(8,128)S(1)} %pad_maximum_fusion.2) | data formatting | bytes 608256 | tf_op jit(solution)/shard_map/concatenate | solution.py:50
  72.0 4.2 %all-to-all-start.3 = ((f32[1,288,4,66]{3,2,0,1:T(4,128)}), f32[1,288,4,66]{3,2,0,1:T(4,128)S(1)}, u32[]{:S(2)}, u32[]{:S(2)}) async-start(f32[1,288,4,66]{3,2,0,1:T(4,128)} %copy.206), calls=%async_computation.3 | async-start | bytes 1179648 | tf_op jit(solution)/shard_map/all_to_all | solution.py:53
  76.2 0.2 reshape_squeeze.10
  76.4 0.3 fusion.60
  76.7 0.2 copy.227
  76.9 0.2 fusion.13
  77.1 0.2 copy.228
  77.2 0.2 reshape_squeeze.11
  77.4 0.4 convolution_bitcast_fusion
  77.8 8.0 %all-to-all-done.3 = f32[1,288,4,66]{3,2,0,1:T(4,128)S(1)} async-done(((f32[1,288,4,66]{3,2,0,1:T(4,128)}), f32[1,288,4,66]{3,2,0,1:T(4,128)S(1)}, u32[]{:S(2)}, u32[]{:S(2)}) %all-to-all-start.3) | async-done | bytes 304160 | tf_op jit(solution)/shard_map/all_to_all | solution.py:53
  85.8 0.5 fusion.58
  86.3 0.5 copy.221
  86.8 0.5 copy.233
  87.3 0.1 copy.237
  87.4 0.1 copy.222
  87.5 0.2 copy.215
  87.7 0.7 fusion.12
  88.5 0.1 fusion.38
  88.6 0.1 reshape.126
  88.7 9.8 %all_to_all.37 = bf16[16,18,256]{2,1,0:T(8,128)(2,1)S(1)} all-to-all(bf16[16,18,256]{2,1,0:T(8,128)(2,1)S(1)} %broadcast_in_dim.74), channel_id=1, replica_groups=mesh['kv'=16,'tp'=8] {'kv'}, dimensions={0} | all-to-all | bytes 294912 | tf_op jit(solution)/shard_map/all_to_all | solution.py:34
  98.6 0.2 convolution_convert_fusion
  98.8 15.0 %all_to_all.38 = bf16[8,36,256]{2,1,0:T(8,128)(2,1)S(1)} all-to-all(bf16[8,36,256]{2,1,0:T(8,128)(2,1)S(1)} %reshape.128), channel_id=1, replica_groups=mesh['kv'=16,'tp'=8] {'tp'}, dimensions={0} | all-to-all | bytes 294912 | tf_op jit(solution)/shard_map/all_to_all | solution.py:62
  113.9 0.6 reduce_sum.72
  (43 shorter events, 0.6 us)
Async XLA Ops:
  0.0 1.2 %copy-start = (bf16[4096,32]{0,1:T(8,128)(2,1)S(1)}, bf16[4096,32]{0,1:T(8,128)(2,1)}, u32[]{:S(2)}) copy-start(bf16[4096,32]{0,1:T(8,128)(2,1)} %param.18) | copy-start | bytes 786436
  0.0 3.9 %copy-start.1 = (bf16[288,256]{1,0:T(8,128)(2,1)S(1)}, bf16[288,256]{1,0:T(8,128)(2,1)}, u32[]{:S(2)}) copy-start(bf16[288,256]{1,0:T(8,128)(2,1)} %param.13) | copy-start | bytes 442372
  0.0 4.8 %copy-start.7 = (f32[256]{0:T(256)S(1)}, f32[256]{0:T(256)}, u32[]{:S(2)}) copy-start(f32[256]{0:T(256)} %param.14) | copy-start | bytes 3076
  0.0 3.9 %copy-start.4 = (bf16[256,256]{1,0:T(8,128)(2,1)S(1)}, bf16[256,256]{1,0:T(8,128)(2,1)}, u32[]{:S(2)}) copy-start(bf16[256,256]{1,0:T(8,128)(2,1)} %param.16) | copy-start | bytes 393220
  0.0 4.7 %copy-start.5 = (bf16[256,256]{1,0:T(8,128)(2,1)S(1)}, bf16[256,256]{1,0:T(8,128)(2,1)}, u32[]{:S(2)}) copy-start(bf16[256,256]{1,0:T(8,128)(2,1)} %param.15) | copy-start | bytes 393220
  7.7 8.6 %copy-start.10 = (s32[12,24]{1,0:T(8,128)S(1)}, s32[12,24]{1,0:T(8,128)}, u32[]{:S(2)}) copy-start(s32[12,24]{1,0:T(8,128)} %param.25) | copy-start | bytes 3460
  7.7 28.6 %all-to-all-start = ((f32[16,18,801]{2,1,0:T(8,128)}), f32[16,18,801]{2,1,0:T(8,128)S(1)}, u32[]{:S(2)}, u32[]{:S(2)}) async-start(f32[16,18,801]{2,1,0:T(8,128)} %pad_maximum_fusion), calls=%async_computation | async-start | bytes 2752512 | tf_op jit(solution)/shard_map/all_to_all | solution.py:17
  16.3 20.4 %copy-start.8 = (f32[32]{0:T(128)S(1)}, f32[32]{0:T(128)}, u32[]{:S(2)}) copy-start(f32[32]{0:T(128)} %param.19) | copy-start | bytes 388
  17.3 36.1 %copy-start.9 = (s32[12]{0:T(128)S(1)}, s32[12]{0:T(128)}, u32[]{:S(2)}) copy-start(s32[12]{0:T(128)} %param.24) | copy-start | bytes 148
  36.4 17.2 %copy-start.2 = (bf16[12,384,256]{2,1,0:T(8,128)(2,1)S(1)}, bf16[12,384,256]{2,1,0:T(8,128)(2,1)}, u32[]{:S(2)}) copy-start(bf16[12,384,256]{2,1,0:T(8,128)(2,1)} %param.21) | copy-start | bytes 7077892
  37.4 11.5 %all-to-all-start.2 = ((bf16[16,2,288]{2,1,0:T(2,128)(2,1)}), bf16[16,2,288]{2,1,0:T(2,128)(2,1)S(1)}, u32[]{:S(2)}, u32[]{:S(2)}) async-start(bf16[16,2,288]{2,1,0:T(2,128)(2,1)} %reshape.131), calls=%async_computation.2 | async-start | bytes 49152 | tf_op jit(solution)/shard_map/all_to_all | solution.py:34
  49.9 13.9 %all-to-all-start.1 = ((bf16[16,18,3,256]{3,1,2,0:T(8,128)(2,1)}), bf16[16,18,3,256]{3,1,2,0:T(8,128)(2,1)S(1)}, u32[]{:S(2)}, u32[]{:S(2)}) async-start(bf16[16,18,3,256]{3,1,2,0:T(8,128)(2,1)} %broadcast_in_dim.67), calls=%async_computation.1 | async-start | bytes 1179648 | tf_op jit(solution)/shard_map/all_to_all | solution.py:34
  60.9 3.3 %copy-start.6 = (f32[12,4,384]{2,1,0:T(4,128)S(1)}, f32[12,4,384]{2,1,0:T(4,128)}, u32[]{:S(2)}) copy-start(f32[12,4,384]{2,1,0:T(4,128)} %param.23) | copy-start | bytes 221188
  72.0 13.8 %all-to-all-start.3 = ((f32[1,288,4,66]{3,2,0,1:T(4,128)}), f32[1,288,4,66]{3,2,0,1:T(4,128)S(1)}, u32[]{:S(2)}, u32[]{:S(2)}) async-start(f32[1,288,4,66]{3,2,0,1:T(4,128)} %copy.206), calls=%async_computation.3 | async-start | bytes 1179648 | tf_op jit(solution)/shard_map/all_to_all | solution.py:53
  86.3 12.3 %copy-start.3 = (bf16[256,256]{1,0:T(8,128)(2,1)S(1)}, bf16[256,256]{1,0:T(8,128)(2,1)}, u32[]{:S(2)}) copy-start(bf16[256,256]{1,0:T(8,128)(2,1)} %param.20) | copy-start | bytes 393220
where the time goes:
time: 115 us; the launch traced here: 114 us
  waiting for transfers between devices  36.2 us (31%)
  blocking collectives  24.8 us (22%)
  starting transfers between devices  21.4 us (19%)
  local copies, waits for them, and re-layouts  14.9 us (13%)
  matrix products  10.5 us (9%)
  other arithmetic  6.17 us (5%)
    all_to_all x1, waiting for transfers between devices, sum_at_owner(): lax.all_to_all(pieces, axis, split_axis=0, concat_axis=0, tiled=True)  19 us
    all_to_all x1, blocking collectives, summed_on_arrival(): pieces = lax.all_to_all(in_blocks(x, dim, devices), axis, 0, 0, tiled=True)  15 us
    all_to_all x1, blocking collectives, copy_for_each(): return lax.all_to_all(copies, axis, split_axis=0, concat_axis=0, tiled=True)  9.78 us
    all_to_all x2, waiting for transfers between devices, copy_for_each(): return lax.all_to_all(copies, axis, split_axis=0, concat_axis=0, tiled=True)  9.21 us
    all_to_all x2, starting transfers between devices, copy_for_each(): return lax.all_to_all(copies, axis, split_axis=0, concat_axis=0, tiled=True)  8.68 us
    all_to_all x1, starting transfers between devices, sum_at_owner(): lax.all_to_all(pieces, axis, split_axis=0, concat_axis=0, tiled=True)  8.55 us
    unnamed x28, local copies, waits for them, and re-layouts  8.19 us
    all_to_all x1, waiting for transfers between devices, in_one_piece_2(): lax.all_to_all(both, axis, split_axis=split_dim, concat_axis=concat_dim,...  7.97 us
  transfers between devices with their start and end apart: 4, of which 4 were waited for; matrix products, arithmetic and copies ran while one was open for 9% of the time, Pallas kernels for 0%

commit v1 on v0

v1 whole, which is shorter than its diff:
```python
import functools

import jax
import jax.numpy as jnp
from jax import lax
from jax.experimental import pallas as pl
from jax.experimental.pallas import tpu as pltpu
from jax.sharding import PartitionSpec as P

MESH = pl.DeviceIdType.MESH
F32 = jnp.float32
BF16 = jnp.bfloat16
NKV = 16
NTP = 8
SEQS = 12
PROPS = 24
POS = 384
HEADS = 4
HEAD_DIM = 64
COLS = HEADS * HEAD_DIM
ROWS = SEQS * PROPS
OUT_ROWS = ROWS // NTP
LANES = 128
FULL_WIDTH = 4096.0
NEG = -1e30
GROUP = 2


def nt_dot(a, b, precision=None):
    return lax.dot_general(
        a, b, (((1,), (1,)), ((), ())), preferred_element_type=F32, precision=precision
    )


def owner_of(seq):
    return seq + 1 + seq // 4


def spread(columns, lane):
    halves = []
    for pair in range(2):
        halves.append(jnp.where(lane < HEAD_DIM, columns[2 * pair], columns[2 * pair + 1]))
    return jnp.concatenate(halves, axis=1)


def diagonal(stacked, lane):
    halves = []
    for pair in range(2):
        even = stacked[(2 * pair) * PROPS : (2 * pair + 1) * PROPS, pair * LANES : (pair + 1) * LANES]
        odd = stacked[
            (2 * pair + 1) * PROPS : (2 * pair + 2) * PROPS, pair * LANES : (pair + 1) * LANES
        ]
        halves.append(jnp.where(lane < HEAD_DIM, even, odd))
    return jnp.concatenate(halves, axis=1)


def by_head(q, wide):
    parts = [
        jnp.where((wide >= h * HEAD_DIM) & (wide < (h + 1) * HEAD_DIM), q, 0.0)
        for h in range(HEADS)
    ]
    return jnp.concatenate(parts, axis=0)


def in_three(x):
    high = x.astype(BF16).astype(F32)
    rest = x - high
    mid = rest.astype(BF16).astype(F32)
    return high, mid, rest - mid


def kernel(
    tokens,
    gain,
    wq,
    wk,
    wv,
    gw,
    bias,
    wo,
    ckeys,
    cvals,
    cdecay,
    lengths,
    parents,
    out_ref,
    v_tok,
    v_gain,
    v_wq,
    v_wk,
    v_wv,
    v_gw,
    v_wo,
    v_ck,
    v_cv,
    v_cd,
    s_q,
    s_k,
    s_v,
    r_q,
    r_k,
    r_v,
    g_q,
    s_mix,
    r_mix,
    g_att,
    f_term,
    s_term,
    r_term,
    load_sem,
    q_send,
    q_recv,
    k_send,
    k_recv,
    v_send,
    v_recv,
    gq_send,
    gq_recv,
    m_send,
    m_recv,
    a_send,
    a_recv,
    t_send,
    t_recv,
):
    kv = lax.axis_index("kv")
    tp = lax.axis_index("tp")
    mine = jnp.where(kv == 0, 0, kv - 1 - lax.div(jnp.maximum(kv - 1, 0), 5))
    mine = jnp.minimum(mine, SEQS - 1)
    is_owner = lax.rem(kv, 5) != 0

    barrier = pltpu.get_barrier_semaphore()
    for r in range(1, NKV):
        pl.semaphore_signal(
            barrier, inc=1, device_id={"kv": lax.rem(kv + r, NKV)}, device_id_type=MESH
        )
    for r in range(1, NTP):
        pl.semaphore_signal(
            barrier, inc=1, device_id={"tp": lax.rem(tp + r, NTP)}, device_id_type=MESH
        )

    gate_rows = gw.at[pl.ds(pl.multiple_of(kv * 256, 256), 256)]
    loads = [
        pltpu.make_async_copy(src, dst, load_sem.at[n])
        for n, (src, dst) in enumerate(
            [
                (tokens, v_tok),
                (gain, v_gain),
                (wq, v_wq),
                (gate_rows, v_gw),
                (wk, v_wk),
                (wv, v_wv),
                (ckeys, v_ck),
                (cdecay, v_cd),
                (cvals, v_cv),
                (wo, v_wo),
            ]
        )
    ]
    for load in loads:
        load.start()
    l_tok, l_gain, l_wq, l_gw, l_wk, l_wv, l_ck, l_cd, l_cv, l_wo = loads

    lane = lax.broadcasted_iota(jnp.int32, (PROPS, LANES), 1)
    wide = lax.broadcasted_iota(jnp.int32, (PROPS, COLS), 1)

    def exchange(src, dst, send, recv, seq):
        return pltpu.make_async_remote_copy(
            src_ref=src.at[seq],
            dst_ref=dst.at[kv],
            send_sem=send.at[seq],
            recv_sem=recv.at[kv],
            device_id={"kv": owner_of(seq)},
            device_id_type=MESH,
        )

    def to_owners(src, dst, send, recv):
        def step(j, carry):
            seq = lax.rem(mine + j, SEQS)

            @pl.when(owner_of(seq) != kv)
            def _():
                exchange(src, dst, send, recv, seq).start()

            return carry

        lax.fori_loop(0, SEQS, step, 0)

    def sent_to_owners(src, dst, send, recv):
        def step(seq, carry):
            @pl.when(owner_of(seq) != kv)
            def _():
                exchange(src, dst, send, recv, seq).wait_send()

            return carry

        lax.fori_loop(0, SEQS, step, 0)

    def arrived(src, dst, send, recv):
        def step(i, carry):
            @pl.when(i != kv)
            def _():
                pltpu.make_async_remote_copy(
                    src_ref=src.at[0],
                    dst_ref=dst.at[i],
                    send_sem=send.at[0],
                    recv_sem=recv.at[i],
                    device_id={"kv": i},
                    device_id_type=MESH,
                ).wait_recv()

            return carry

        lax.fori_loop(0, NKV, step, 0)

    def gather_copy(buf, send, recv, peer, slot, seq):
        return pltpu.make_async_remote_copy(
            src_ref=buf.at[seq],
            dst_ref=buf.at[seq],
            send_sem=send.at[slot],
            recv_sem=recv.at[seq],
            device_id={"kv": peer},
            device_id_type=MESH,
        )

    def to_all(buf, send, recv):
        def step(r, carry):
            gather_copy(buf, send, recv, lax.rem(kv + r, NKV), r, mine).start()
            return carry

        lax.fori_loop(1, NKV, step, 0)

    def sent_to_all(buf, send, recv):
        def step(r, carry):
            gather_copy(buf, send, recv, lax.rem(kv + r, NKV), r, mine).wait_send()
            return carry

        lax.fori_loop(1, NKV, step, 0)

    def await_seq(buf, send, recv, seq):
        @pl.when(owner_of(seq) != kv)
        def _():
            gather_copy(buf, send, recv, owner_of(seq), 0, seq).wait_recv()

    l_tok.wait()
    l_gain.wait()
    x = v_tok[...].astype(F32)
    squares = jnp.sum(x * x, axis=1, keepdims=True)
    normed = (x * v_gain[...]).astype(BF16)
    l_wq.wait()
    s_q[:, :, 0:COLS] = jnp.dot(normed, v_wq[...], preferred_element_type=F32).reshape(
        SEQS, PROPS, COLS
    )
    l_gw.wait()
    pick = lax.broadcasted_iota(jnp.int32, (32, LANES), 0) == (
        tp * HEADS + lax.broadcasted_iota(jnp.int32, (32, LANES), 1)
    )
    pick = pick & (lax.broadcasted_iota(jnp.int32, (32, LANES), 1) < HEADS)
    own_gates = jnp.dot(
        v_gw[...], pick.astype(F32).astype(BF16), preferred_element_type=F32
    ).astype(BF16)
    extra = jnp.dot(normed, own_gates, preferred_element_type=F32)
    lane_rows = lax.broadcasted_iota(jnp.int32, (ROWS, LANES), 1)
    extra = jnp.where(lane_rows < HEADS, extra, squares)
    s_q[:, :, COLS:] = extra.reshape(SEQS, PROPS, LANES)

    pl.semaphore_wait(barrier, NKV - 1 + NTP - 1)
    to_owners(s_q, r_q, q_send, q_recv)

    l_wk.wait()
    s_k[...] = jnp.dot(normed, v_wk[...], preferred_element_type=F32).reshape(SEQS, PROPS, COLS)
    to_owners(s_k, r_k, k_send, k_recv)
    l_wv.wait()
    s_v[...] = jnp.dot(normed, v_wv[...], preferred_element_type=F32).reshape(SEQS, PROPS, COLS)

    @pl.when(is_owner)
    def _():
        r_q[kv] = s_q[mine]
        arrived(s_q, r_q, q_send, q_recv)
        total = r_q[0]
        for i in range(1, NKV):
            total = total + r_q[i]
        s_q[mine] = total
        inverse = lax.rsqrt(total[:, COLS + HEADS : COLS + HEADS + 1] / FULL_WIDTH + 1e-6)
        g_q[mine] = (inverse * total[:, :COLS]).astype(BF16)
        to_all(g_q, gq_send, gq_recv)

    to_owners(s_v, r_v, v_send, v_recv)

    l_ck.wait()
    l_cd.wait()
    l_cv.wait()
    position = kv * POS + lax.broadcasted_iota(jnp.int32, (1, POS), 1)

    def attend(seq):
        q = by_head(g_q[seq].astype(F32) * (HEAD_DIM**-0.5), wide).astype(BF16)
        scores = nt_dot(q, v_ck[seq])
        live = position < lengths[seq]
        parts = []
        for h in range(HEADS):
            decay = jnp.where(live, v_cd[seq, h : h + 1, :], NEG)
            parts.append(scores[h * PROPS : (h + 1) * PROPS] + decay)
        scores = jnp.concatenate(parts, axis=0)
        top = jnp.max(scores, axis=1, keepdims=True)
        weights = jnp.exp(scores - top)
        total = jnp.sum(weights, axis=1, keepdims=True)
        mix = jnp.dot(weights.astype(BF16), v_cv[seq], preferred_element_type=F32)
        stats = jnp.zeros((PROPS, LANES), F32)
        for h in range(HEADS):
            rows = slice(h * PROPS, (h + 1) * PROPS)
            for n, piece in enumerate(in_three(top[rows]) + in_three(total[rows])):
                stats = jnp.where(lane == n * HEADS + h, piece, stats)
        s_mix[seq] = jnp.concatenate([diagonal(mix, lane), stats], axis=1).astype(BF16)

    def attend_group(j, carry):
        seqs = [lax.rem(mine + j * GROUP + u, SEQS) for u in range(GROUP)]
        for seq in seqs:
            await_seq(g_q, gq_send, gq_recv, seq)
        for seq in seqs:
            attend(seq)
        for seq in seqs:

            @pl.when(owner_of(seq) != kv)
            def _():
                exchange(s_mix, r_mix, m_send, m_recv, seq).start()

        return carry

    lax.fori_loop(0, SEQS // GROUP, attend_group, 0)

    @pl.when(is_owner)
    def _():
        r_k[kv] = s_k[mine]
        r_v[kv] = s_v[mine]
        r_mix[kv] = s_mix[mine]
        summed = s_q[mine]
        inverse = lax.rsqrt(summed[:, COLS + HEADS : COLS + HEADS + 1] / FULL_WIDTH + 1e-6)
        gates = inverse * summed[:, COLS:]
        shift = jnp.zeros((PROPS, LANES), F32)
        for h in range(HEADS):
            shift = jnp.where(lane == h, bias[tp * HEADS + h], shift)
        gates = gates + shift
        log_gates = jnp.minimum(gates, 0.0) - jnp.log1p(jnp.exp(-jnp.abs(gates)))
        square = (PROPS, PROPS)
        older = lax.broadcasted_iota(jnp.int32, square, 0)
        younger = lax.broadcasted_iota(jnp.int32, square, 1)
        linked = (older == parents[pl.ds(mine, 1), :]) | (older == younger)
        up = linked.astype(F32)
        for _ in range(5):
            closed = up.astype(BF16)
            up = jnp.minimum(jnp.dot(closed, closed, preferred_element_type=F32), 1.0)
        eye = (older == younger).astype(F32)
        ancestry = nt_dot(eye.astype(BF16), up.astype(BF16))
        path = jnp.dot(
            ancestry, log_gates, preferred_element_type=F32, precision=lax.Precision.HIGHEST
        )
        padded = jnp.concatenate([path, jnp.zeros((LANES - PROPS, LANES), F32)], axis=0)
        path_rows = padded.T

        arrived(s_k, r_k, k_send, k_recv)
        new_keys = r_k[0]
        for i in range(1, NKV):
            new_keys = new_keys + r_k[i]
        new_keys = (inverse * new_keys).astype(BF16)
        q = by_head(g_q[mine].astype(F32) * (HEAD_DIM**-0.5), wide).astype(BF16)
        scores = nt_dot(q, new_keys)
        parts = []
        for h in range(HEADS):
            part = scores[h * PROPS : (h + 1) * PROPS] - path_rows[h : h + 1, :PROPS]
            parts.append(jnp.where(ancestry > 0.5, part, NEG))
        scores = jnp.concatenate(parts, axis=0)
        tree_top = jnp.max(scores, axis=1, keepdims=True)
        weights = jnp.exp(scores - tree_top)
        tree_total = jnp.sum(weights, axis=1, keepdims=True)
        arrived(s_v, r_v, v_send, v_recv)
        new_values = r_v[0]
        for i in range(1, NKV):
            new_values = new_values + r_v[i]
        new_values = (inverse * new_values).astype(BF16)
        tree_mix = diagonal(
            jnp.dot(weights.astype(BF16), new_values, preferred_element_type=F32), lane
        )
        tree_stats = jnp.zeros((PROPS, LANES), F32)
        for h in range(HEADS):
            rows = slice(h * PROPS, (h + 1) * PROPS)
            tree_stats = jnp.where(lane == h, tree_top[rows], tree_stats)
            tree_stats = jnp.where(lane == 3 * HEADS + h, tree_total[rows], tree_stats)

        arrived(s_mix, r_mix, m_send, m_recv)

        def stats_of(i):
            packed = r_mix[i, :, COLS:].astype(F32)
            one = pltpu.roll(packed, LANES - HEADS, 1)
            two = pltpu.roll(packed, LANES - 2 * HEADS, 1)
            return packed + (one + two)

        stats = [stats_of(i) for i in range(NKV)] + [tree_stats]
        best = functools.reduce(jnp.maximum, stats)
        factors = [jnp.exp(s - best) for s in stats]
        denominator = functools.reduce(
            jnp.add,
            [pltpu.roll(s, LANES - 3 * HEADS, 1) * f for s, f in zip(stats, factors)],
        )
        numerator = jnp.zeros((PROPS, COLS), F32)
        for i in range(NKV + 1):
            values = r_mix[i, :, :COLS].astype(F32) if i < NKV else tree_mix
            numerator = numerator + values * spread(
                [factors[i][:, h : h + 1] for h in range(HEADS)], lane
            )
        below = spread([denominator[:, h : h + 1] for h in range(HEADS)], lane)
        g_att[mine] = (numerator / below).astype(BF16)
        to_all(g_att, a_send, a_recv)

    l_wo.wait()

    def await_attended(seq, carry):
        await_seq(g_att, a_send, a_recv, seq)
        return carry

    lax.fori_loop(0, SEQS, await_attended, 0)
    attended = jnp.concatenate([g_att[s].astype(F32) for s in range(SEQS)], axis=0).astype(BF16)
    f_term[...] = jnp.dot(attended, v_wo[...], preferred_element_type=F32)

    def term_copy(to):
        return pltpu.make_async_remote_copy(
            src_ref=s_term.at[to],
            dst_ref=r_term.at[tp],
            send_sem=t_send.at[to],
            recv_sem=t_recv.at[tp],
            device_id={"tp": to},
            device_id_type=MESH,
        )

    for t in range(NTP):
        s_term[t] = f_term[t * OUT_ROWS : (t + 1) * OUT_ROWS, :].astype(BF16)

    def send_term(r, carry):
        term_copy(lax.rem(tp + r, NTP)).start()
        return carry

    lax.fori_loop(1, NTP, send_term, 0)
    r_term[tp] = s_term[tp]

    def term_arrived(r, carry):
        source = lax.rem(tp + r, NTP)
        pltpu.make_async_remote_copy(
            src_ref=s_term.at[source],
            dst_ref=r_term.at[source],
            send_sem=t_send.at[source],
            recv_sem=t_recv.at[source],
            device_id={"tp": source},
            device_id_type=MESH,
        ).wait_recv()
        return carry

    lax.fori_loop(1, NTP, term_arrived, 0)
    mixed = r_term[0].astype(F32)
    for t in range(1, NTP):
        mixed = mixed + r_term[t].astype(F32)
    out_ref[...] = mixed.astype(BF16)

    sent_to_owners(s_q, r_q, q_send, q_recv)
    sent_to_owners(s_k, r_k, k_send, k_recv)
    sent_to_owners(s_v, r_v, v_send, v_recv)
    sent_to_owners(s_mix, r_mix, m_send, m_recv)

    @pl.when(is_owner)
    def _():
        sent_to_all(g_q, gq_send, gq_recv)
        sent_to_all(g_att, a_send, a_recv)

    def term_sent(r, carry):
        term_copy(lax.rem(tp + r, NTP)).wait_send()
        return carry

    lax.fori_loop(1, NTP, term_sent, 0)


def body(
    tokens,
    norm_gain,
    query_weight,
    key_weight,
    value_weight,
    gate_weight,
    gate_bias,
    out_weight,
    cache_keys,
    cache_values,
    cache_decay,
    lengths,
    parents,
):
    anywhere = pl.BlockSpec(memory_space=pl.ANY)
    scalars = pl.BlockSpec(memory_space=pltpu.SMEM)
    vector = pl.BlockSpec(memory_space=pltpu.VMEM)
    dma = pltpu.SemaphoreType.DMA
    return pl.pallas_call(
        kernel,
        out_shape=jax.ShapeDtypeStruct((OUT_ROWS, COLS), BF16),
        in_specs=[anywhere] * 6 + [scalars] + [anywhere] * 4 + [scalars, vector],
        out_specs=vector,
        scratch_shapes=[
            pltpu.VMEM((ROWS, COLS), BF16),
            pltpu.VMEM((1, COLS), F32),
            pltpu.VMEM((COLS, COLS), BF16),
            pltpu.VMEM((COLS, COLS), BF16),
            pltpu.VMEM((COLS, COLS), BF16),
            pltpu.VMEM((COLS, 32), BF16),
            pltpu.VMEM((COLS, COLS), BF16),
            pltpu.VMEM((SEQS, POS, COLS), BF16),
            pltpu.VMEM((SEQS, POS, COLS), BF16),
            pltpu.VMEM((SEQS, HEADS, POS), F32),
            pltpu.VMEM((SEQS, PROPS, COLS + LANES), F32),
            pltpu.VMEM((SEQS, PROPS, COLS), F32),
            pltpu.VMEM((SEQS, PROPS, COLS), F32),
            pltpu.VMEM((NKV, PROPS, COLS + LANES), F32),
            pltpu.VMEM((NKV, PROPS, COLS), F32),
            pltpu.VMEM((NKV, PROPS, COLS), F32),
            pltpu.VMEM((SEQS, PROPS, COLS), BF16),
            pltpu.VMEM((SEQS, PROPS, COLS + LANES), BF16),
            pltpu.VMEM((NKV, PROPS, COLS + LANES), BF16),
            pltpu.VMEM((SEQS, PROPS, COLS), BF16),
            pltpu.VMEM((ROWS, COLS), F32),
            pltpu.VMEM((NTP, OUT_ROWS, COLS), BF16),
            pltpu.VMEM((NTP, OUT_ROWS, COLS), BF16),
            dma((10,)),
            dma((SEQS,)),
            dma((NKV,)),
            dma((SEQS,)),
            dma((NKV,)),
            dma((SEQS,)),
            dma((NKV,)),
            dma((NKV,)),
            dma((SEQS,)),
            dma((SEQS,)),
            dma((NKV,)),
            dma((NKV,)),
            dma((SEQS,)),
            dma((NTP,)),
            dma((NTP,)),
        ],
        compiler_params=pltpu.CompilerParams(
            collective_id=0, has_side_effects=True, vmem_limit_bytes=60 * 1024 * 1024
        ),
        name="tree_attention",
    )(
        tokens,
        norm_gain.reshape(1, -1),
        query_weight,
        key_weight,
        value_weight,
        gate_weight,
        gate_bias,
        out_weight,
        cache_keys,
        cache_values,
        cache_decay,
        lengths,
        parents,
    )


def solution(mesh):
    in_specs = (
        P(None, "kv"),
        P("kv"),
        P("kv", "tp"),
        P("kv", "tp"),
        P("kv", "tp"),
        P(),
        P(),
        P("tp", "kv"),
        P(None, "kv", "tp"),
        P(None, "kv", "tp"),
        P(None, "tp", "kv"),
        P(),
        P(),
    )
    out_specs = P("tp", "kv")
    return jax.shard_map(body, mesh=mesh, in_specs=in_specs, out_specs=out_specs, check_vma=False)
```

time: 115 us -> 53.4 us (0.46)
  Pallas kernels: 0 us -> 49.5 us
  waiting for transfers between devices: 36.2 us -> 0 us
  blocking collectives: 24.8 us -> 0 us
  starting transfers between devices: 21.4 us -> 0 us
  local copies, waits for them, and re-layouts: 14.9 us -> 3.62 us
  matrix products: 10.5 us -> 0 us
  other arithmetic: 6.17 us -> 0 us
    pallas_call x0 -> x1, Pallas kernels: none -> 49.5 us  [body(): pl.pallas_call(kernel, out_shape=jax.ShapeDtypeStruct((OUT_ROWS, COLS), B...]
    all_to_all x4 -> x0, waiting for transfers between devices: 36.2 us -> none  [the longest x1 19 us: sum_at_owner(): lax.all_to_all(pieces, axis, split_axis=0, concat_axis=0, tiled=True)]
    all_to_all x2 -> x0, blocking collectives: 24.8 us -> none  [the longest x1 15 us: summed_on_arrival(): pieces = lax.all_to_all(in_blocks(x, dim, devices), axis, 0, 0, tiled=True)]
    all_to_all x4 -> x0, starting transfers between devices: 21.4 us -> none  [the longest x2 8.68 us: copy_for_each(): return lax.all_to_all(copies, axis, split_axis=0, concat_axis=0, tiled=True)]
    dot_general x13 -> x0, matrix products: 10.5 us -> none  [the longest x1 2.65 us: body(): jnp.einsum('snhj,sjhd->snhd', weights.astype(jnp.bfloat16), values, prefe...]
    unnamed x28 -> x2, local copies, waits for them, and re-layouts: 8.19 us -> 3.62 us
    reduce_sum x7 -> x0, other arithmetic: 3.41 us -> none  [the longest x1 1.14 us: body(): squares = jnp.sum(xf * xf, axis=1)]
    concatenate x5 -> x0, local copies, waits for them, and re-layouts: 2.4 us -> none  [the longest x4 1.21 us: in_one_piece(): both = jnp.concatenate(columns, axis=along)]
  transfers between devices with their start and end apart: 4 -> 0, of which waited for: 4 -> 0; matrix products, arithmetic and copies ran while one was open for 9% -> 0% of each run, Pallas kernels for 0% -> 0%
where the time goes in v1:
time: 53.4 us; the launch traced here: 53.1 us
  Pallas kernels  49.5 us (93%)
  local copies, waits for them, and re-layouts  3.62 us (7%)
    pallas_call x1, Pallas kernels, body(): pl.pallas_call(kernel, out_shape=jax.ShapeDtypeStruct((OUT_ROWS, COLS), B...  49.5 us
    unnamed x2, local copies, waits for them, and re-layouts  3.62 us

profile of v1, /device:TPU:1, one launch (start us, length us, event | category | flops | bytes accessed | tf_op | source)
XLA Modules:
  0.0 53.1 jit_solution(10573060639334571619)
XLA Ops:
  0.0 2.3 %copy.14.gw = bf16[4096,32]{1,0:T(8,128)(2,1)} copy(bf16[4096,32]{0,1:T(8,128)(2,1)} %param.18) | data formatting | bytes 524288 | tf_op args[5]
  2.3 49.5 %tree_attention.1 = bf16[36,256]{1,0:T(8,128)(2,1)} custom-call(bf16[288,256]{1,0:T(8,128)(2,1)} %tokens.1, f32[1,256]{1,0:T(1,128)} %bitcast.1, bf16[256,256]{1,0:T(8,128)(2,1)} %wq.1, bf16[256,256]{1,0:T(8,128)(2,1)} %wk.1, bf16[256,256]{1,0:T(8,128)(2,1)} %wv.1, bf16[4096,32]{1,0:T(8,128)(2,1)} %copy.14.gw, f32[32]{0:T(128)} %bias.1, ...), custom_call_target="tpu_custom_call" | custom-call | tf_op jit(solution)/shard_map/tree_attention/pallas_call | solution.py:498
  51.8 1.3 %copy.16 = bf16[36,256]{1,0:T(8,128)(2,1)} copy(bf16[36,256]{1,0:T(8,128)(2,1)} %tree_attention.1) | data formatting | bytes 36864

commit v2 on v1

--- a/solution.py
+++ b/solution.py
@@ -23,7 +23,7 @@
 LANES = 128
 FULL_WIDTH = 4096.0
 NEG = -1e30
-GROUP = 2
+GROUP = 3
 
 
 def nt_dot(a, b, precision=None):
@@ -106,7 +106,6 @@
     g_att,
     f_term,
     s_term,
-    r_term,
     load_sem,
     q_send,
     q_recv,
@@ -139,7 +138,7 @@
             barrier, inc=1, device_id={"tp": lax.rem(tp + r, NTP)}, device_id_type=MESH
         )
 
-    gate_rows = gw.at[pl.ds(pl.multiple_of(kv * 256, 256), 256)]
+    gate_cols = gw.at[:, pl.ds(pl.multiple_of(kv * COLS, COLS), COLS)]
     loads = [
         pltpu.make_async_copy(src, dst, load_sem.at[n])
         for n, (src, dst) in enumerate(
@@ -147,7 +146,7 @@
                 (tokens, v_tok),
                 (gain, v_gain),
                 (wq, v_wq),
-                (gate_rows, v_gw),
+                (gate_cols, v_gw),
                 (wk, v_wk),
                 (wv, v_wv),
                 (ckeys, v_ck),
@@ -242,6 +241,8 @@
         def _():
             gather_copy(buf, send, recv, owner_of(seq), 0, seq).wait_recv()
 
+    pending = []
+
     l_tok.wait()
     l_gain.wait()
     x = v_tok[...].astype(F32)
@@ -252,26 +253,26 @@
         SEQS, PROPS, COLS
     )
     l_gw.wait()
-    pick = lax.broadcasted_iota(jnp.int32, (32, LANES), 0) == (
-        tp * HEADS + lax.broadcasted_iota(jnp.int32, (32, LANES), 1)
-    )
-    pick = pick & (lax.broadcasted_iota(jnp.int32, (32, LANES), 1) < HEADS)
+    pick_row = lax.broadcasted_iota(jnp.int32, (LANES, 32), 0)
+    pick_col = lax.broadcasted_iota(jnp.int32, (LANES, 32), 1)
+    pick = (pick_col == tp * HEADS + pick_row) & (pick_row < HEADS)
     own_gates = jnp.dot(
-        v_gw[...], pick.astype(F32).astype(BF16), preferred_element_type=F32
+        pick.astype(F32).astype(BF16), v_gw[...], preferred_element_type=F32
     ).astype(BF16)
-    extra = jnp.dot(normed, own_gates, preferred_element_type=F32)
+    extra = nt_dot(normed, own_gates)
     lane_rows = lax.broadcasted_iota(jnp.int32, (ROWS, LANES), 1)
     extra = jnp.where(lane_rows < HEADS, extra, squares)
     s_q[:, :, COLS:] = extra.reshape(SEQS, PROPS, LANES)
 
     pl.semaphore_wait(barrier, NKV - 1 + NTP - 1)
     to_owners(s_q, r_q, q_send, q_recv)
+    pending.append(lambda: sent_to_owners(s_q, r_q, q_send, q_recv))
 
     l_wk.wait()
     s_k[...] = jnp.dot(normed, v_wk[...], preferred_element_type=F32).reshape(SEQS, PROPS, COLS)
-    to_owners(s_k, r_k, k_send, k_recv)
     l_wv.wait()
-    s_v[...] = jnp.dot(normed, v_wv[...], preferred_element_type=F32).reshape(SEQS, PROPS, COLS)
+    new = jnp.dot(normed, v_wv[...], preferred_element_type=F32)
+    s_v[...] = new.astype(BF16).reshape(SEQS, PROPS, COLS)
 
     @pl.when(is_owner)
     def _():
@@ -285,7 +286,11 @@
         g_q[mine] = (inverse * total[:, :COLS]).astype(BF16)
         to_all(g_q, gq_send, gq_recv)
 
+    pending.append(lambda: pl.when(is_owner)(lambda: sent_to_all(g_q, gq_send, gq_recv)))
+    to_owners(s_k, r_k, k_send, k_recv)
+    pending.append(lambda: sent_to_owners(s_k, r_k, k_send, k_recv))
     to_owners(s_v, r_v, v_send, v_recv)
+    pending.append(lambda: sent_to_owners(s_v, r_v, v_send, v_recv))
 
     l_ck.wait()
     l_cd.wait()
@@ -313,7 +318,7 @@
         s_mix[seq] = jnp.concatenate([diagonal(mix, lane), stats], axis=1).astype(BF16)
 
     def attend_group(j, carry):
-        seqs = [lax.rem(mine + j * GROUP + u, SEQS) for u in range(GROUP)]
+        seqs = [lax.rem(mine + SEQS - j * GROUP - u, SEQS) for u in range(GROUP)]
         for seq in seqs:
             await_seq(g_q, gq_send, gq_recv, seq)
         for seq in seqs:
@@ -328,6 +333,7 @@
 
     lax.fori_loop(0, SEQS // GROUP, attend_group, 0)
 
+    pending.append(lambda: sent_to_owners(s_mix, r_mix, m_send, m_recv))
     @pl.when(is_owner)
     def _():
         r_k[kv] = s_k[mine]
@@ -373,9 +379,9 @@
         weights = jnp.exp(scores - tree_top)
         tree_total = jnp.sum(weights, axis=1, keepdims=True)
         arrived(s_v, r_v, v_send, v_recv)
-        new_values = r_v[0]
+        new_values = r_v[0].astype(F32)
         for i in range(1, NKV):
-            new_values = new_values + r_v[i]
+            new_values = new_values + r_v[i].astype(F32)
         new_values = (inverse * new_values).astype(BF16)
         tree_mix = diagonal(
             jnp.dot(weights.astype(BF16), new_values, preferred_element_type=F32), lane
@@ -411,6 +417,7 @@
         g_att[mine] = (numerator / below).astype(BF16)
         to_all(g_att, a_send, a_recv)
 
+    pending.append(lambda: pl.when(is_owner)(lambda: sent_to_all(g_att, a_send, a_recv)))
     l_wo.wait()
 
     def await_attended(seq, carry):
@@ -421,12 +428,12 @@
     attended = jnp.concatenate([g_att[s].astype(F32) for s in range(SEQS)], axis=0).astype(BF16)
     f_term[...] = jnp.dot(attended, v_wo[...], preferred_element_type=F32)
 
-    def term_copy(to):
+    def term_copy(to, source):
         return pltpu.make_async_remote_copy(
             src_ref=s_term.at[to],
-            dst_ref=r_term.at[tp],
+            dst_ref=out_ref.at[source],
             send_sem=t_send.at[to],
-            recv_sem=t_recv.at[tp],
+            recv_sem=t_recv.at[source],
             device_id={"tp": to},
             device_id_type=MESH,
         )
@@ -435,45 +442,26 @@
         s_term[t] = f_term[t * OUT_ROWS : (t + 1) * OUT_ROWS, :].astype(BF16)
 
     def send_term(r, carry):
-        term_copy(lax.rem(tp + r, NTP)).start()
+        term_copy(lax.rem(tp + r, NTP), tp).start()
         return carry
 
     lax.fori_loop(1, NTP, send_term, 0)
-    r_term[tp] = s_term[tp]
+    out_ref[tp] = s_term[tp]
 
     def term_arrived(r, carry):
         source = lax.rem(tp + r, NTP)
-        pltpu.make_async_remote_copy(
-            src_ref=s_term.at[source],
-            dst_ref=r_term.at[source],
-            send_sem=t_send.at[source],
-            recv_sem=t_recv.at[source],
-            device_id={"tp": source},
-            device_id_type=MESH,
-        ).wait_recv()
+        term_copy(source, source).wait_recv()
         return carry
 
     lax.fori_loop(1, NTP, term_arrived, 0)
-    mixed = r_term[0].astype(F32)
-    for t in range(1, NTP):
-        mixed = mixed + r_term[t].astype(F32)
-    out_ref[...] = mixed.astype(BF16)
-
-    sent_to_owners(s_q, r_q, q_send, q_recv)
-    sent_to_owners(s_k, r_k, k_send, k_recv)
-    sent_to_owners(s_v, r_v, v_send, v_recv)
-    sent_to_owners(s_mix, r_mix, m_send, m_recv)
-
-    @pl.when(is_owner)
-    def _():
-        sent_to_all(g_q, gq_send, gq_recv)
-        sent_to_all(g_att, a_send, a_recv)
 
     def term_sent(r, carry):
-        term_copy(lax.rem(tp + r, NTP)).wait_send()
+        term_copy(lax.rem(tp + r, NTP), tp).wait_send()
         return carry
 
     lax.fori_loop(1, NTP, term_sent, 0)
+    for wait in pending:
+        wait()
 
 
 def body(
@@ -495,9 +483,9 @@
     scalars = pl.BlockSpec(memory_space=pltpu.SMEM)
     vector = pl.BlockSpec(memory_space=pltpu.VMEM)
     dma = pltpu.SemaphoreType.DMA
-    return pl.pallas_call(
+    terms = pl.pallas_call(
         kernel,
-        out_shape=jax.ShapeDtypeStruct((OUT_ROWS, COLS), BF16),
+        out_shape=jax.ShapeDtypeStruct((NTP, OUT_ROWS, COLS), BF16),
         in_specs=[anywhere] * 6 + [scalars] + [anywhere] * 4 + [scalars, vector],
         out_specs=vector,
         scratch_shapes=[
@@ -506,23 +494,22 @@
             pltpu.VMEM((COLS, COLS), BF16),
             pltpu.VMEM((COLS, COLS), BF16),
             pltpu.VMEM((COLS, COLS), BF16),
-            pltpu.VMEM((COLS, 32), BF16),
+            pltpu.VMEM((32, COLS), BF16),
             pltpu.VMEM((COLS, COLS), BF16),
             pltpu.VMEM((SEQS, POS, COLS), BF16),
             pltpu.VMEM((SEQS, POS, COLS), BF16),
             pltpu.VMEM((SEQS, HEADS, POS), F32),
             pltpu.VMEM((SEQS, PROPS, COLS + LANES), F32),
             pltpu.VMEM((SEQS, PROPS, COLS), F32),
-            pltpu.VMEM((SEQS, PROPS, COLS), F32),
+            pltpu.VMEM((SEQS, PROPS, COLS), BF16),
             pltpu.VMEM((NKV, PROPS, COLS + LANES), F32),
             pltpu.VMEM((NKV, PROPS, COLS), F32),
-            pltpu.VMEM((NKV, PROPS, COLS), F32),
+            pltpu.VMEM((NKV, PROPS, COLS), BF16),
             pltpu.VMEM((SEQS, PROPS, COLS), BF16),
             pltpu.VMEM((SEQS, PROPS, COLS + LANES), BF16),
             pltpu.VMEM((NKV, PROPS, COLS + LANES), BF16),
             pltpu.VMEM((SEQS, PROPS, COLS), BF16),
             pltpu.VMEM((ROWS, COLS), F32),
-            pltpu.VMEM((NTP, OUT_ROWS, COLS), BF16),
             pltpu.VMEM((NTP, OUT_ROWS, COLS), BF16),
             dma((10,)),
             dma((SEQS,)),
@@ -550,7 +537,7 @@
         query_weight,
         key_weight,
         value_weight,
-        gate_weight,
+        gate_weight.T,
         gate_bias,
         out_weight,
         cache_keys,
@@ -559,6 +546,7 @@
         lengths,
         parents,
     )
+    return jnp.sum(terms.astype(F32), axis=0).astype(BF16)
 
 
 def solution(mesh):

time: 53.4 us -> 45.9 us (0.86)
  Pallas kernels: 49.5 us -> 44.2 us
  local copies, waits for them, and re-layouts: 3.62 us -> 0 us
  other arithmetic: 0 us -> 1.56 us
    pallas_call x1, Pallas kernels: 49.5 us -> 44.2 us  [body(): pl.pallas_call(kernel, out_shape=jax.ShapeDtypeStruct((NTP, OUT_ROWS, COL...]
    unnamed x2 -> x0, local copies, waits for them, and re-layouts: 3.62 us -> none
    reduce_sum x0 -> x1, other arithmetic: none -> 1.56 us  [body(): return jnp.sum(terms.astype(F32), axis=0).astype(BF16)]
where the time goes in v2:
time: 45.9 us; the launch traced here: 45.8 us
  Pallas kernels  44.2 us (96%)
  other arithmetic  1.56 us (3%)
    pallas_call x1, Pallas kernels, body(): pl.pallas_call(kernel, out_shape=jax.ShapeDtypeStruct((NTP, OUT_ROWS, COL...  44.2 us
    reduce_sum x1, other arithmetic, body(): return jnp.sum(terms.astype(F32), axis=0).astype(BF16)  1.56 us

profile of v2, /device:TPU:1, one launch (start us, length us, event | category | flops | bytes accessed | tf_op | source)
XLA Modules:
  0.0 45.8 jit_solution(8730882190195347564)
XLA Ops:
  0.0 44.2 %tree_attention.1 = bf16[8,36,256]{2,1,0:T(8,128)(2,1)} custom-call(bf16[288,256]{1,0:T(8,128)(2,1)} %tokens.1, f32[1,256]{1,0:T(1,128)} %bitcast.3, bf16[256,256]{1,0:T(8,128)(2,1)} %wq.1, bf16[256,256]{1,0:T(8,128)(2,1)} %wk.1, bf16[256,256]{1,0:T(8,128)(2,1)} %wv.1, bf16[32,4096]{1,0:T(8,128)(2,1)} %bitcast.2, f32[32]{0:T(128)} %bias.1, ...), custom_call_target="tpu_custom_call" | custom-call | tf_op jit(solution)/shard_map/tree_attention/pallas_call | solution.py:486
  44.2 1.6 %reduce_sum.12 = bf16[36,256]{1,0:T(8,128)(2,1)} reduce(bf16[8,36,256]{2,1,0:T(8,128)(2,1)} %tree_attention.1, bf16[]{:T(256)} %constant.2.clone.1), dimensions={0}, to_apply=%region_0.0 | reduce | flops 64512 | bytes 165890 | tf_op jit(solution)/shard_map/reduce_sum | solution.py:549

commit v3 on v2

--- a/solution.py
+++ b/solution.py
@@ -24,6 +24,7 @@
 FULL_WIDTH = 4096.0
 NEG = -1e30
 GROUP = 3
+HALF = 16
 
 
 def nt_dot(a, b, precision=None):
@@ -32,8 +33,26 @@
     )
 
 
+def below(value, count):
+    return jnp.where(value >= count, value - count, value)
+
+
+def third(value):
+    part = (
+        jnp.where(value >= 3, 1, 0) + jnp.where(value >= 6, 1, 0) + jnp.where(value >= 9, 1, 0)
+    )
+    return part, value - 3 * part
+
+
 def owner_of(seq):
-    return seq + 1 + seq // 4
+    group, place = third(seq)
+    row = below(group + 4 - place, 4)
+    return 4 * row + place + jnp.where(place >= row, 1, 0)
+
+
+def seq_at(index):
+    row, place = third(index)
+    return 3 * below(row + place, 4) + place
 
 
 def spread(columns, lane):
@@ -94,6 +113,9 @@
     v_ck,
     v_cv,
     v_cd,
+    v_len,
+    v_bias,
+    v_par,
     s_q,
     s_k,
     s_v,
@@ -103,9 +125,10 @@
     g_q,
     s_mix,
     r_mix,
-    g_att,
-    f_term,
-    s_term,
+    s_att,
+    s_half,
+    r_att,
+    r_half,
     load_sem,
     q_send,
     q_recv,
@@ -119,24 +142,22 @@
     m_recv,
     a_send,
     a_recv,
-    t_send,
-    t_recv,
+    w_send,
+    w_recv,
 ):
     kv = lax.axis_index("kv")
     tp = lax.axis_index("tp")
-    mine = jnp.where(kv == 0, 0, kv - 1 - lax.div(jnp.maximum(kv - 1, 0), 5))
-    mine = jnp.minimum(mine, SEQS - 1)
-    is_owner = lax.rem(kv, 5) != 0
-
-    barrier = pltpu.get_barrier_semaphore()
-    for r in range(1, NKV):
-        pl.semaphore_signal(
-            barrier, inc=1, device_id={"kv": lax.rem(kv + r, NKV)}, device_id_type=MESH
-        )
-    for r in range(1, NTP):
-        pl.semaphore_signal(
-            barrier, inc=1, device_id={"tp": lax.rem(tp + r, NTP)}, device_id_type=MESH
-        )
+    row, column = lax.div(kv, 4), lax.rem(kv, 4)
+    is_owner = row != column
+    index = 3 * row + jnp.minimum(jnp.where(column > row, column - 1, column), 2)
+    mine = seq_at(index)
+    out_group, out_place = third(mine)
+    whole_to = 2 * out_group + jnp.where(out_place == 2, 1, 0)
+    is_whole = is_owner & (out_place != 1)
+    is_half = is_owner & (out_place == 1)
+    out_third = lax.div(tp, 2)
+    odd = tp - 2 * out_third
+    sources = [owner_of(3 * out_third + 2 * odd), owner_of(3 * out_third + 1)]
 
     gate_cols = gw.at[:, pl.ds(pl.multiple_of(kv * COLS, COLS), COLS)]
     loads = [
@@ -152,13 +173,38 @@
                 (ckeys, v_ck),
                 (cdecay, v_cd),
                 (cvals, v_cv),
-                (wo, v_wo),
+                (wo, v_wo.at[tp]),
+                (lengths, v_len),
+                (bias, v_bias),
+                (parents, v_par),
             ]
         )
     ]
     for load in loads:
         load.start()
-    l_tok, l_gain, l_wq, l_gw, l_wk, l_wv, l_ck, l_cd, l_cv, l_wo = loads
+    l_tok, l_gain, l_wq, l_gw, l_wk, l_wv, l_ck, l_cd, l_cv, l_wo, l_len, l_bias, l_par = loads
+
+    barrier = pltpu.get_barrier_semaphore()
+    for r in range(1, NKV):
+        pl.semaphore_signal(
+            barrier, inc=1, device_id={"kv": below(kv + r, NKV)}, device_id_type=MESH
+        )
+    for r in range(1, NTP):
+        pl.semaphore_signal(
+            barrier, inc=1, device_id={"tp": below(tp + r, NTP)}, device_id_type=MESH
+        )
+    greeted = NKV - 1 + NTP - 1
+    greeted = greeted + jnp.where(is_whole, NKV, 0) + jnp.where(is_half, 2 * NKV, 0)
+    greeted = greeted - jnp.where(is_whole & (tp == whole_to), 1, 0)
+    greeted = greeted - jnp.where(is_half & (out_third == out_group), 1, 0)
+    for source in sources:
+        for group in range(NTP):
+
+            @pl.when((source != kv) | (tp != group))
+            def _():
+                pl.semaphore_signal(
+                    barrier, inc=1, device_id={"kv": source, "tp": group}, device_id_type=MESH
+                )
 
     lane = lax.broadcasted_iota(jnp.int32, (PROPS, LANES), 1)
     wide = lax.broadcasted_iota(jnp.int32, (PROPS, COLS), 1)
@@ -175,7 +221,7 @@
 
     def to_owners(src, dst, send, recv):
         def step(j, carry):
-            seq = lax.rem(mine + j, SEQS)
+            seq = seq_at(below(index + j, SEQS))
 
             @pl.when(owner_of(seq) != kv)
             def _():
@@ -186,14 +232,11 @@
         lax.fori_loop(0, SEQS, step, 0)
 
     def sent_to_owners(src, dst, send, recv):
-        def step(seq, carry):
+        for seq in range(SEQS):
+
             @pl.when(owner_of(seq) != kv)
             def _():
                 exchange(src, dst, send, recv, seq).wait_send()
-
-            return carry
-
-        lax.fori_loop(0, SEQS, step, 0)
 
     def arrived(src, dst, send, recv):
         def step(i, carry):
@@ -224,17 +267,34 @@
 
     def to_all(buf, send, recv):
         def step(r, carry):
-            gather_copy(buf, send, recv, lax.rem(kv + r, NKV), r, mine).start()
+            gather_copy(buf, send, recv, below(kv + r, NKV), r, mine).start()
             return carry
 
         lax.fori_loop(1, NKV, step, 0)
 
     def sent_to_all(buf, send, recv):
-        def step(r, carry):
-            gather_copy(buf, send, recv, lax.rem(kv + r, NKV), r, mine).wait_send()
-            return carry
-
-        lax.fori_loop(1, NKV, step, 0)
+        for r in range(1, NKV):
+            gather_copy(buf, send, recv, below(kv + r, NKV), r, mine).wait_send()
+
+    def whole_copy(r):
+        return pltpu.make_async_remote_copy(
+            src_ref=s_att,
+            dst_ref=r_att.at[tp],
+            send_sem=a_send.at[r],
+            recv_sem=a_recv.at[tp],
+            device_id={"kv": below(kv + r, NKV), "tp": whole_to},
+            device_id_type=MESH,
+        )
+
+    def half_copy(r, c):
+        return pltpu.make_async_remote_copy(
+            src_ref=s_half.at[c],
+            dst_ref=r_half.at[tp],
+            send_sem=a_send.at[NKV * c + r],
+            recv_sem=a_recv.at[NTP + tp],
+            device_id={"kv": below(kv + r, NKV), "tp": 2 * out_group + c},
+            device_id_type=MESH,
+        )
 
     def await_seq(buf, send, recv, seq):
         @pl.when(owner_of(seq) != kv)
@@ -264,9 +324,36 @@
     extra = jnp.where(lane_rows < HEADS, extra, squares)
     s_q[:, :, COLS:] = extra.reshape(SEQS, PROPS, LANES)
 
-    pl.semaphore_wait(barrier, NKV - 1 + NTP - 1)
+    pl.semaphore_wait(barrier, greeted)
     to_owners(s_q, r_q, q_send, q_recv)
     pending.append(lambda: sent_to_owners(s_q, r_q, q_send, q_recv))
+
+    def weight_copy(to, source):
+        return pltpu.make_async_remote_copy(
+            src_ref=v_wo.at[source],
+            dst_ref=v_wo.at[source],
+            send_sem=w_send.at[to],
+            recv_sem=w_recv.at[source],
+            device_id={"tp": to},
+            device_id_type=MESH,
+        )
+
+    def send_weight(r, carry):
+        weight_copy(below(tp + r, NTP), tp).start()
+        return carry
+
+    def weight_sent(r, carry):
+        weight_copy(below(tp + r, NTP), tp).wait_send()
+        return carry
+
+    def weight_arrived(r, carry):
+        source = below(tp + r, NTP)
+        weight_copy(source, source).wait_recv()
+        return carry
+
+    l_wo.wait()
+    lax.fori_loop(1, NTP, send_weight, 0)
+    pending.append(lambda: lax.fori_loop(1, NTP, weight_sent, 0))
 
     l_wk.wait()
     s_k[...] = jnp.dot(normed, v_wk[...], preferred_element_type=F32).reshape(SEQS, PROPS, COLS)
@@ -294,13 +381,16 @@
 
     l_ck.wait()
     l_cd.wait()
+    l_len.wait()
+    l_bias.wait()
+    l_par.wait()
     l_cv.wait()
     position = kv * POS + lax.broadcasted_iota(jnp.int32, (1, POS), 1)
 
     def attend(seq):
         q = by_head(g_q[seq].astype(F32) * (HEAD_DIM**-0.5), wide).astype(BF16)
         scores = nt_dot(q, v_ck[seq])
-        live = position < lengths[seq]
+        live = position < v_len[seq]
         parts = []
         for h in range(HEADS):
             decay = jnp.where(live, v_cd[seq, h : h + 1, :], NEG)
@@ -318,7 +408,7 @@
         s_mix[seq] = jnp.concatenate([diagonal(mix, lane), stats], axis=1).astype(BF16)
 
     def attend_group(j, carry):
-        seqs = [lax.rem(mine + SEQS - j * GROUP - u, SEQS) for u in range(GROUP)]
+        seqs = [seq_at(below(index + SEQS - j * GROUP - u, SEQS)) for u in range(GROUP)]
         for seq in seqs:
             await_seq(g_q, gq_send, gq_recv, seq)
         for seq in seqs:
@@ -344,13 +434,13 @@
         gates = inverse * summed[:, COLS:]
         shift = jnp.zeros((PROPS, LANES), F32)
         for h in range(HEADS):
-            shift = jnp.where(lane == h, bias[tp * HEADS + h], shift)
+            shift = jnp.where(lane == h, v_bias[tp * HEADS + h], shift)
         gates = gates + shift
         log_gates = jnp.minimum(gates, 0.0) - jnp.log1p(jnp.exp(-jnp.abs(gates)))
         square = (PROPS, PROPS)
         older = lax.broadcasted_iota(jnp.int32, square, 0)
         younger = lax.broadcasted_iota(jnp.int32, square, 1)
-        linked = (older == parents[pl.ds(mine, 1), :]) | (older == younger)
+        linked = (older == v_par[pl.ds(mine, 1), :]) | (older == younger)
         up = linked.astype(F32)
         for _ in range(5):
             closed = up.astype(BF16)
@@ -413,55 +503,110 @@
             numerator = numerator + values * spread(
                 [factors[i][:, h : h + 1] for h in range(HEADS)], lane
             )
-        below = spread([denominator[:, h : h + 1] for h in range(HEADS)], lane)
-        g_att[mine] = (numerator / below).astype(BF16)
-        to_all(g_att, a_send, a_recv)
-
-    pending.append(lambda: pl.when(is_owner)(lambda: sent_to_all(g_att, a_send, a_recv)))
-    l_wo.wait()
-
-    def await_attended(seq, carry):
-        await_seq(g_att, a_send, a_recv, seq)
-        return carry
-
-    lax.fori_loop(0, SEQS, await_attended, 0)
-    attended = jnp.concatenate([g_att[s].astype(F32) for s in range(SEQS)], axis=0).astype(BF16)
-    f_term[...] = jnp.dot(attended, v_wo[...], preferred_element_type=F32)
-
-    def term_copy(to, source):
-        return pltpu.make_async_remote_copy(
-            src_ref=s_term.at[to],
-            dst_ref=out_ref.at[source],
-            send_sem=t_send.at[to],
-            recv_sem=t_recv.at[source],
-            device_id={"tp": to},
-            device_id_type=MESH,
-        )
-
-    for t in range(NTP):
-        s_term[t] = f_term[t * OUT_ROWS : (t + 1) * OUT_ROWS, :].astype(BF16)
-
-    def send_term(r, carry):
-        term_copy(lax.rem(tp + r, NTP), tp).start()
-        return carry
-
-    lax.fori_loop(1, NTP, send_term, 0)
-    out_ref[tp] = s_term[tp]
-
-    def term_arrived(r, carry):
-        source = lax.rem(tp + r, NTP)
-        term_copy(source, source).wait_recv()
-        return carry
-
-    lax.fori_loop(1, NTP, term_arrived, 0)
-
-    def term_sent(r, carry):
-        term_copy(lax.rem(tp + r, NTP), tp).wait_send()
-        return carry
-
-    lax.fori_loop(1, NTP, term_sent, 0)
+        under = spread([denominator[:, h : h + 1] for h in range(HEADS)], lane)
+        attended = numerator / under
+
+        @pl.when(out_place != 1)
+        def _():
+            s_att[...] = attended.astype(BF16)
+
+            def step(r, carry):
+                whole_copy(r).start()
+                return carry
+
+            lax.fori_loop(1, NKV, step, 0)
+
+            @pl.when(tp != whole_to)
+            def _():
+                whole_copy(0).start()
+
+            @pl.when(tp == whole_to)
+            def _():
+                r_att[tp] = s_att[...]
+
+        @pl.when(out_place == 1)
+        def _():
+            s_half[0] = attended[:HALF].astype(BF16)
+            s_half[1] = attended[PROPS - HALF :].astype(BF16)
+
+            def step(r, carry):
+                half_copy(r, 0).start()
+                half_copy(r, 1).start()
+                return carry
+
+            lax.fori_loop(1, NKV, step, 0)
+            for c in range(2):
+
+                @pl.when(tp != 2 * out_group + c)
+                def _():
+                    half_copy(0, c).start()
+
+                @pl.when(tp == 2 * out_group + c)
+                def _():
+                    r_half[tp] = s_half[c]
+
+    def scattered():
+        @pl.when(is_whole)
+        def _():
+            for r in range(1, NKV):
+                whole_copy(r).wait_send()
+
+            @pl.when(tp != whole_to)
+            def _():
+                whole_copy(0).wait_send()
+
+        @pl.when(is_half)
+        def _():
+            for c in range(2):
+                for r in range(1, NKV):
+                    half_copy(r, c).wait_send()
+
+                @pl.when(tp != 2 * out_group + c)
+                def _():
+                    half_copy(0, c).wait_send()
+
+    lax.fori_loop(1, NTP, weight_arrived, 0)
     for wait in pending:
         wait()
+
+    for group in range(NTP):
+
+        @pl.when((sources[0] != kv) | (tp != group))
+        def _():
+            pltpu.make_async_remote_copy(
+                src_ref=s_att,
+                dst_ref=r_att.at[group],
+                send_sem=a_send.at[0],
+                recv_sem=a_recv.at[group],
+                device_id={"kv": sources[0], "tp": group},
+                device_id_type=MESH,
+            ).wait_recv()
+
+        @pl.when((sources[1] != kv) | (tp != group))
+        def _():
+            pltpu.make_async_remote_copy(
+                src_ref=s_half.at[0],
+                dst_ref=r_half.at[group],
+                send_sem=a_send.at[0],
+                recv_sem=a_recv.at[NTP + group],
+                device_id={"kv": sources[1], "tp": group},
+                device_id_type=MESH,
+            ).wait_recv()
+
+    mixed = jnp.zeros((PROPS + HALF, COLS), F32)
+    for group in range(NTP):
+        whole, half = r_att[group].astype(F32), r_half[group].astype(F32)
+        both = jnp.where(
+            odd == 1,
+            jnp.concatenate([half, whole], axis=0),
+            jnp.concatenate([whole, half], axis=0),
+        )
+        term = jnp.dot(both.astype(BF16), v_wo[group], preferred_element_type=F32)
+        mixed = mixed + term.astype(BF16).astype(F32)
+    out_ref[...] = jnp.where(
+        odd == 1, mixed[PROPS + HALF - OUT_ROWS :], mixed[:OUT_ROWS]
+    ).astype(BF16)
+    scattered()
 
 
 def body(
@@ -480,13 +625,12 @@
     parents,
 ):
     anywhere = pl.BlockSpec(memory_space=pl.ANY)
-    scalars = pl.BlockSpec(memory_space=pltpu.SMEM)
     vector = pl.BlockSpec(memory_space=pltpu.VMEM)
     dma = pltpu.SemaphoreType.DMA
-    terms = pl.pallas_call(
+    return pl.pallas_call(
         kernel,
-        out_shape=jax.ShapeDtypeStruct((NTP, OUT_ROWS, COLS), BF16),
-        in_specs=[anywhere] * 6 + [scalars] + [anywhere] * 4 + [scalars, vector],
+        out_shape=jax.ShapeDtypeStruct((OUT_ROWS, COLS), BF16),
+        in_specs=[anywhere] * 13,
         out_specs=vector,
         scratch_shapes=[
             pltpu.VMEM((ROWS, COLS), BF16),
@@ -495,10 +639,13 @@
             pltpu.VMEM((COLS, COLS), BF16),
             pltpu.VMEM((COLS, COLS), BF16),
             pltpu.VMEM((32, COLS), BF16),
-            pltpu.VMEM((COLS, COLS), BF16),
+            pltpu.VMEM((NTP, COLS, COLS), BF16),
             pltpu.VMEM((SEQS, POS, COLS), BF16),
             pltpu.VMEM((SEQS, POS, COLS), BF16),
             pltpu.VMEM((SEQS, HEADS, POS), F32),
+            pltpu.SMEM((SEQS,), jnp.int32),
+            pltpu.SMEM((NTP * HEADS,), F32),
+            pltpu.VMEM((SEQS, PROPS), jnp.int32),
             pltpu.VMEM((SEQS, PROPS, COLS + LANES), F32),
             pltpu.VMEM((SEQS, PROPS, COLS), F32),
             pltpu.VMEM((SEQS, PROPS, COLS), BF16),
@@ -508,10 +655,11 @@
             pltpu.VMEM((SEQS, PROPS, COLS), BF16),
             pltpu.VMEM((SEQS, PROPS, COLS + LANES), BF16),
             pltpu.VMEM((NKV, PROPS, COLS + LANES), BF16),
-            pltpu.VMEM((SEQS, PROPS, COLS), BF16),
-            pltpu.VMEM((ROWS, COLS), F32),
-            pltpu.VMEM((NTP, OUT_ROWS, COLS), BF16),
-            dma((10,)),
+            pltpu.VMEM((PROPS, COLS), BF16),
+            pltpu.VMEM((2, HALF, COLS), BF16),
+            pltpu.VMEM((NTP, PROPS, COLS), BF16),
+            pltpu.VMEM((NTP, HALF, COLS), BF16),
+            dma((13,)),
             dma((SEQS,)),
             dma((NKV,)),
             dma((SEQS,)),
@@ -522,8 +670,8 @@
             dma((SEQS,)),
             dma((SEQS,)),
             dma((NKV,)),
-            dma((NKV,)),
-            dma((SEQS,)),
+            dma((2 * NKV,)),
+            dma((2 * NTP,)),
             dma((NTP,)),
             dma((NTP,)),
         ],
@@ -546,7 +694,6 @@
         lengths,
         parents,
     )
-    return jnp.sum(terms.astype(F32), axis=0).astype(BF16)
 
 
 def solution(mesh):

time: 45.9 us -> 42.2 us (0.919)
  Pallas kernels: 44.2 us -> 40.7 us
  other arithmetic: 1.56 us -> 0 us
  local copies, waits for them, and re-layouts: 0 us -> 1.34 us
    pallas_call x1, Pallas kernels: 44.2 us -> 40.7 us  [body(): pl.pallas_call(kernel, out_shape=jax.ShapeDtypeStruct((OUT_ROWS, COLS), B...]
    reduce_sum x1 -> x0, other arithmetic: 1.56 us -> none  [body(): return jnp.sum(terms.astype(F32), axis=0).astype(BF16)]
    unnamed x0 -> x1, local copies, waits for them, and re-layouts: none -> 1.34 us
where the time goes in v3:
time: 42.2 us; the launch traced here: 42 us
  Pallas kernels  40.7 us (96%)
  local copies, waits for them, and re-layouts  1.34 us (3%)
    pallas_call x1, Pallas kernels, body(): pl.pallas_call(kernel, out_shape=jax.ShapeDtypeStruct((OUT_ROWS, COLS), B...  40.7 us
    unnamed x1, local copies, waits for them, and re-layouts  1.34 us

profile of v3, /device:TPU:1, one launch (start us, length us, event | category | flops | bytes accessed | tf_op | source)
XLA Modules:
  0.0 42.0 jit_solution(15454738845854061958)
XLA Ops:
  0.0 40.7 %tree_attention.1 = bf16[36,256]{1,0:T(8,128)(2,1)} custom-call(bf16[288,256]{1,0:T(8,128)(2,1)} %tokens.1, f32[1,256]{1,0:T(1,128)} %bitcast.3, bf16[256,256]{1,0:T(8,128)(2,1)} %wq.1, bf16[256,256]{1,0:T(8,128)(2,1)} %wk.1, bf16[256,256]{1,0:T(8,128)(2,1)} %wv.1, bf16[32,4096]{1,0:T(8,128)(2,1)} %bitcast.2, f32[32]{0:T(128)} %bias.1, bf16[256,256]{1,0:T(8,128)(2,1)} %wo.1, ...), custom_call_target="tpu_custom_call" | custom-call | tf_op jit(solution)/shard_map/tree_attention/pallas_call | solution.py:630
  40.7 1.3 %copy.15 = bf16[36,256]{1,0:T(8,128)(2,1)} copy(bf16[36,256]{1,0:T(8,128)(2,1)} %tree_attention.1) | data formatting | bytes 36864

commit v4 on v3

--- a/solution.py
+++ b/solution.py
@@ -25,6 +25,11 @@
 NEG = -1e30
 GROUP = 3
 HALF = 16
+FEW = 8
+FAR_FIRST = sorted(
+    [(z, x) for z in range(4) for x in range(4) if z or x],
+    key=lambda d: -sum(min(n, 4 - n) for n in d),
+)
 
 
 def nt_dot(a, b, precision=None):
@@ -79,13 +84,6 @@
         for h in range(HEADS)
     ]
     return jnp.concatenate(parts, axis=0)
-
-
-def in_three(x):
-    high = x.astype(BF16).astype(F32)
-    rest = x - high
-    mid = rest.astype(BF16).astype(F32)
-    return high, mid, rest - mid
 
 
 def kernel(
@@ -117,14 +115,22 @@
     v_bias,
     v_par,
     s_q,
+    s_sq,
+    s_x,
     s_k,
     s_v,
     r_q,
+    r_sq,
+    r_x,
     r_k,
     r_v,
     g_q,
+    i_row,
+    i_col,
     s_mix,
+    s_stat,
     r_mix,
+    r_stat,
     s_att,
     s_half,
     r_att,
@@ -132,6 +138,10 @@
     load_sem,
     q_send,
     q_recv,
+    z_send,
+    z_recv,
+    x_send,
+    x_recv,
     k_send,
     k_recv,
     v_send,
@@ -140,6 +150,8 @@
     gq_recv,
     m_send,
     m_recv,
+    y_send,
+    y_recv,
     a_send,
     a_recv,
     w_send,
@@ -219,17 +231,17 @@
             device_id_type=MESH,
         )
 
+    def at_distance(z, x):
+        return below(row + z, 4), below(column + x, 4)
+
     def to_owners(src, dst, send, recv):
-        def step(j, carry):
-            seq = seq_at(below(index + j, SEQS))
-
-            @pl.when(owner_of(seq) != kv)
+        for distance in FAR_FIRST:
+            z, x = at_distance(*distance)
+
+            @pl.when(z != x)
             def _():
+                seq = seq_at(3 * z + jnp.where(x > z, x - 1, x))
                 exchange(src, dst, send, recv, seq).start()
-
-            return carry
-
-        lax.fori_loop(0, SEQS, step, 0)
 
     def sent_to_owners(src, dst, send, recv):
         for seq in range(SEQS):
@@ -266,33 +278,32 @@
         )
 
     def to_all(buf, send, recv):
-        def step(r, carry):
+        for r in range(1, NKV):
             gather_copy(buf, send, recv, below(kv + r, NKV), r, mine).start()
-            return carry
-
-        lax.fori_loop(1, NKV, step, 0)
 
     def sent_to_all(buf, send, recv):
         for r in range(1, NKV):
             gather_copy(buf, send, recv, below(kv + r, NKV), r, mine).wait_send()
 
-    def whole_copy(r):
+    def whole_copy(distance):
+        z, x = at_distance(*distance)
         return pltpu.make_async_remote_copy(
             src_ref=s_att,
             dst_ref=r_att.at[tp],
-            send_sem=a_send.at[r],
+            send_sem=a_send.at[4 * distance[0] + distance[1]],
             recv_sem=a_recv.at[tp],
-            device_id={"kv": below(kv + r, NKV), "tp": whole_to},
+            device_id={"kv": 4 * z + x, "tp": whole_to},
             device_id_type=MESH,
         )
 
-    def half_copy(r, c):
+    def half_copy(distance, c):
+        z, x = at_distance(*distance)
         return pltpu.make_async_remote_copy(
             src_ref=s_half.at[c],
             dst_ref=r_half.at[tp],
-            send_sem=a_send.at[NKV * c + r],
+            send_sem=a_send.at[NKV * c + 4 * distance[0] + distance[1]],
             recv_sem=a_recv.at[NTP + tp],
-            device_id={"kv": below(kv + r, NKV), "tp": 2 * out_group + c},
+            device_id={"kv": 4 * z + x, "tp": 2 * out_group + c},
             device_id_type=MESH,
         )
 
@@ -306,26 +317,37 @@
     l_tok.wait()
     l_gain.wait()
     x = v_tok[...].astype(F32)
-    squares = jnp.sum(x * x, axis=1, keepdims=True)
     normed = (x * v_gain[...]).astype(BF16)
     l_wq.wait()
-    s_q[:, :, 0:COLS] = jnp.dot(normed, v_wq[...], preferred_element_type=F32).reshape(
-        SEQS, PROPS, COLS
-    )
+    s_q[...] = jnp.dot(normed, v_wq[...], preferred_element_type=F32).reshape(SEQS, PROPS, COLS)
+    squares = x * x
+    high = squares.astype(BF16)
+    low = (squares - high.astype(F32)).astype(BF16)
+    ones = jnp.ones((16, COLS), BF16)
+    square_rows = nt_dot(ones, high) + nt_dot(ones, low)
     l_gw.wait()
-    pick_row = lax.broadcasted_iota(jnp.int32, (LANES, 32), 0)
-    pick_col = lax.broadcasted_iota(jnp.int32, (LANES, 32), 1)
+    pick_row = lax.broadcasted_iota(jnp.int32, (16, 32), 0)
+    pick_col = lax.broadcasted_iota(jnp.int32, (16, 32), 1)
     pick = (pick_col == tp * HEADS + pick_row) & (pick_row < HEADS)
     own_gates = jnp.dot(
         pick.astype(F32).astype(BF16), v_gw[...], preferred_element_type=F32
     ).astype(BF16)
-    extra = nt_dot(normed, own_gates)
-    lane_rows = lax.broadcasted_iota(jnp.int32, (ROWS, LANES), 1)
-    extra = jnp.where(lane_rows < HEADS, extra, squares)
-    s_q[:, :, COLS:] = extra.reshape(SEQS, PROPS, LANES)
+    rows = jnp.where(
+        lax.broadcasted_iota(jnp.int32, (FEW, ROWS), 0) < HEADS,
+        nt_dot(own_gates, normed)[:FEW],
+        square_rows[:FEW],
+    )
+    rows = jnp.concatenate([rows, jnp.zeros((FEW, 3 * LANES - ROWS), F32)], axis=1)
+    for seq in range(SEQS):
+        shift = (3 * LANES - seq * PROPS) % (3 * LANES)
+        turned = pltpu.roll(rows, shift, 1) if shift else rows
+        s_x[seq] = turned[:, :LANES]
+        s_sq[seq] = turned[HEADS : HEADS + 1, :LANES]
 
     pl.semaphore_wait(barrier, greeted)
+    to_owners(s_sq, r_sq, z_send, z_recv)
     to_owners(s_q, r_q, q_send, q_recv)
+    pending.append(lambda: sent_to_owners(s_sq, r_sq, z_send, z_recv))
     pending.append(lambda: sent_to_owners(s_q, r_q, q_send, q_recv))
 
     def weight_copy(to, source):
@@ -364,16 +386,25 @@
     @pl.when(is_owner)
     def _():
         r_q[kv] = s_q[mine]
+        r_sq[kv] = s_sq[mine]
+        arrived(s_sq, r_sq, z_send, z_recv)
+        summed = r_sq[0]
+        for i in range(1, NKV):
+            summed = summed + r_sq[i]
+        i_row[...] = lax.rsqrt(summed / FULL_WIDTH + 1e-6)
+        on_diagonal = lane == lax.broadcasted_iota(jnp.int32, (PROPS, LANES), 0)
+        inverse = jnp.sum(jnp.where(on_diagonal, i_row[...], 0.0), axis=1, keepdims=True)
+        i_col[...] = jnp.broadcast_to(inverse, (PROPS, LANES))
         arrived(s_q, r_q, q_send, q_recv)
         total = r_q[0]
         for i in range(1, NKV):
             total = total + r_q[i]
-        s_q[mine] = total
-        inverse = lax.rsqrt(total[:, COLS + HEADS : COLS + HEADS + 1] / FULL_WIDTH + 1e-6)
-        g_q[mine] = (inverse * total[:, :COLS]).astype(BF16)
+        g_q[mine] = (inverse * total).astype(BF16)
         to_all(g_q, gq_send, gq_recv)
 
     pending.append(lambda: pl.when(is_owner)(lambda: sent_to_all(g_q, gq_send, gq_recv)))
+    to_owners(s_x, r_x, x_send, x_recv)
+    pending.append(lambda: sent_to_owners(s_x, r_x, x_send, x_recv))
     to_owners(s_k, r_k, k_send, k_recv)
     pending.append(lambda: sent_to_owners(s_k, r_k, k_send, k_recv))
     to_owners(s_v, r_v, v_send, v_recv)
@@ -386,6 +417,15 @@
     l_par.wait()
     l_cv.wait()
     position = kv * POS + lax.broadcasted_iota(jnp.int32, (1, POS), 1)
+
+    def stat_rows(top, total):
+        stats = jnp.zeros((PROPS, LANES), F32)
+        for h in range(HEADS):
+            own = slice(h * PROPS, (h + 1) * PROPS)
+            stats = jnp.where(lane == h, top[own], stats)
+            stats = jnp.where(lane == HEADS + h, total[own], stats)
+        padded = jnp.concatenate([stats, jnp.zeros((LANES - PROPS, LANES), F32)], axis=0)
+        return padded.T[:FEW]
 
     def attend(seq):
         q = by_head(g_q[seq].astype(F32) * (HEAD_DIM**-0.5), wide).astype(BF16)
@@ -400,12 +440,8 @@
         weights = jnp.exp(scores - top)
         total = jnp.sum(weights, axis=1, keepdims=True)
         mix = jnp.dot(weights.astype(BF16), v_cv[seq], preferred_element_type=F32)
-        stats = jnp.zeros((PROPS, LANES), F32)
-        for h in range(HEADS):
-            rows = slice(h * PROPS, (h + 1) * PROPS)
-            for n, piece in enumerate(in_three(top[rows]) + in_three(total[rows])):
-                stats = jnp.where(lane == n * HEADS + h, piece, stats)
-        s_mix[seq] = jnp.concatenate([diagonal(mix, lane), stats], axis=1).astype(BF16)
+        s_mix[seq] = diagonal(mix, lane).astype(BF16)
+        s_stat[seq] = stat_rows(top, total)
 
     def attend_group(j, carry):
         seqs = [seq_at(below(index + SEQS - j * GROUP - u, SEQS)) for u in range(GROUP)]
@@ -417,6 +453,7 @@
 
             @pl.when(owner_of(seq) != kv)
             def _():
+                exchange(s_stat, r_stat, y_send, y_recv, seq).start()
                 exchange(s_mix, r_mix, m_send, m_recv, seq).start()
 
         return carry
@@ -424,18 +461,24 @@
     lax.fori_loop(0, SEQS // GROUP, attend_group, 0)
 
     pending.append(lambda: sent_to_owners(s_mix, r_mix, m_send, m_recv))
+    pending.append(lambda: sent_to_owners(s_stat, r_stat, y_send, y_recv))
     @pl.when(is_owner)
     def _():
         r_k[kv] = s_k[mine]
         r_v[kv] = s_v[mine]
         r_mix[kv] = s_mix[mine]
-        summed = s_q[mine]
-        inverse = lax.rsqrt(summed[:, COLS + HEADS : COLS + HEADS + 1] / FULL_WIDTH + 1e-6)
-        gates = inverse * summed[:, COLS:]
-        shift = jnp.zeros((PROPS, LANES), F32)
+        r_stat[kv] = s_stat[mine]
+        r_x[kv] = s_x[mine]
+        inverse = i_col[:, 0:1]
+        head_row = lax.broadcasted_iota(jnp.int32, (FEW, LANES), 0)
+        shift = jnp.zeros((FEW, LANES), F32)
         for h in range(HEADS):
-            shift = jnp.where(lane == h, v_bias[tp * HEADS + h], shift)
-        gates = gates + shift
+            shift = jnp.where(head_row == h, v_bias[tp * HEADS + h], shift)
+        arrived(s_x, r_x, x_send, x_recv)
+        gates = r_x[0]
+        for i in range(1, NKV):
+            gates = gates + r_x[i]
+        gates = i_row[...] * gates + shift
         log_gates = jnp.minimum(gates, 0.0) - jnp.log1p(jnp.exp(-jnp.abs(gates)))
         square = (PROPS, PROPS)
         older = lax.broadcasted_iota(jnp.int32, square, 0)
@@ -447,11 +490,9 @@
             up = jnp.minimum(jnp.dot(closed, closed, preferred_element_type=F32), 1.0)
         eye = (older == younger).astype(F32)
         ancestry = nt_dot(eye.astype(BF16), up.astype(BF16))
-        path = jnp.dot(
-            ancestry, log_gates, preferred_element_type=F32, precision=lax.Precision.HIGHEST
-        )
-        padded = jnp.concatenate([path, jnp.zeros((LANES - PROPS, LANES), F32)], axis=0)
-        path_rows = padded.T
+        path_rows = jnp.dot(
+            log_gates[:, :PROPS], up, preferred_element_type=F32, precision=lax.Precision.HIGHEST
+        )
 
         arrived(s_k, r_k, k_send, k_recv)
         new_keys = r_k[0]
@@ -462,7 +503,7 @@
         scores = nt_dot(q, new_keys)
         parts = []
         for h in range(HEADS):
-            part = scores[h * PROPS : (h + 1) * PROPS] - path_rows[h : h + 1, :PROPS]
+            part = scores[h * PROPS : (h + 1) * PROPS] - path_rows[h : h + 1]
             parts.append(jnp.where(ancestry > 0.5, part, NEG))
         scores = jnp.concatenate(parts, axis=0)
         tree_top = jnp.max(scores, axis=1, keepdims=True)
@@ -476,49 +517,36 @@
         tree_mix = diagonal(
             jnp.dot(weights.astype(BF16), new_values, preferred_element_type=F32), lane
         )
-        tree_stats = jnp.zeros((PROPS, LANES), F32)
-        for h in range(HEADS):
-            rows = slice(h * PROPS, (h + 1) * PROPS)
-            tree_stats = jnp.where(lane == h, tree_top[rows], tree_stats)
-            tree_stats = jnp.where(lane == 3 * HEADS + h, tree_total[rows], tree_stats)
-
-        arrived(s_mix, r_mix, m_send, m_recv)
-
-        def stats_of(i):
-            packed = r_mix[i, :, COLS:].astype(F32)
-            one = pltpu.roll(packed, LANES - HEADS, 1)
-            two = pltpu.roll(packed, LANES - 2 * HEADS, 1)
-            return packed + (one + two)
-
-        stats = [stats_of(i) for i in range(NKV)] + [tree_stats]
+        tree_stats = stat_rows(tree_top, tree_total)
+
+        arrived(s_stat, r_stat, y_send, y_recv)
+        stats = [r_stat[i] for i in range(NKV)] + [tree_stats]
         best = functools.reduce(jnp.maximum, stats)
         factors = [jnp.exp(s - best) for s in stats]
         denominator = functools.reduce(
-            jnp.add,
-            [pltpu.roll(s, LANES - 3 * HEADS, 1) * f for s, f in zip(stats, factors)],
-        )
-        numerator = jnp.zeros((PROPS, COLS), F32)
-        for i in range(NKV + 1):
-            values = r_mix[i, :, :COLS].astype(F32) if i < NKV else tree_mix
-            numerator = numerator + values * spread(
-                [factors[i][:, h : h + 1] for h in range(HEADS)], lane
-            )
-        under = spread([denominator[:, h : h + 1] for h in range(HEADS)], lane)
-        attended = numerator / under
+            jnp.add, [pltpu.roll(s, HEADS, 0) * f for s, f in zip(stats, factors)]
+        )
+        under = 1.0 / denominator
+        columns = jnp.concatenate([f * under for f in factors[:NKV]], axis=0).T[:PROPS]
+        tree_columns = jnp.concatenate(
+            [factors[NKV] * under, jnp.zeros((LANES - FEW, LANES), F32)], axis=0
+        ).T[:PROPS]
+        attended = tree_mix * spread([tree_columns[:, h : h + 1] for h in range(HEADS)], lane)
+        arrived(s_mix, r_mix, m_send, m_recv)
+        for i in range(NKV):
+            shares = [columns[:, FEW * i + h : FEW * i + h + 1] for h in range(HEADS)]
+            attended = attended + r_mix[i].astype(F32) * spread(shares, lane)
 
         @pl.when(out_place != 1)
         def _():
             s_att[...] = attended.astype(BF16)
 
-            def step(r, carry):
-                whole_copy(r).start()
-                return carry
-
-            lax.fori_loop(1, NKV, step, 0)
+            for distance in FAR_FIRST:
+                whole_copy(distance).start()
 
             @pl.when(tp != whole_to)
             def _():
-                whole_copy(0).start()
+                whole_copy((0, 0)).start()
 
             @pl.when(tp == whole_to)
             def _():
@@ -529,17 +557,14 @@
             s_half[0] = attended[:HALF].astype(BF16)
             s_half[1] = attended[PROPS - HALF :].astype(BF16)
 
-            def step(r, carry):
-                half_copy(r, 0).start()
-                half_copy(r, 1).start()
-                return carry
-
-            lax.fori_loop(1, NKV, step, 0)
+            for distance in FAR_FIRST:
+                half_copy(distance, 0).start()
+                half_copy(distance, 1).start()
             for c in range(2):
 
                 @pl.when(tp != 2 * out_group + c)
                 def _():
-                    half_copy(0, c).start()
+                    half_copy((0, 0), c).start()
 
                 @pl.when(tp == 2 * out_group + c)
                 def _():
@@ -548,22 +573,22 @@
     def scattered():
         @pl.when(is_whole)
         def _():
-            for r in range(1, NKV):
-                whole_copy(r).wait_send()
+            for distance in FAR_FIRST:
+                whole_copy(distance).wait_send()
 
             @pl.when(tp != whole_to)
             def _():
-                whole_copy(0).wait_send()
+                whole_copy((0, 0)).wait_send()
 
         @pl.when(is_half)
         def _():
             for c in range(2):
-                for r in range(1, NKV):
-                    half_copy(r, c).wait_send()
+                for distance in FAR_FIRST:
+                    half_copy(distance, c).wait_send()
 
                 @pl.when(tp != 2 * out_group + c)
                 def _():
-                    half_copy(0, c).wait_send()
+                    half_copy((0, 0), c).wait_send()
 
     lax.fori_loop(1, NTP, weight_arrived, 0)
     for wait in pending:
@@ -646,15 +671,23 @@
             pltpu.SMEM((SEQS,), jnp.int32),
             pltpu.SMEM((NTP * HEADS,), F32),
             pltpu.VMEM((SEQS, PROPS), jnp.int32),
-            pltpu.VMEM((SEQS, PROPS, COLS + LANES), F32),
+            pltpu.VMEM((SEQS, PROPS, COLS), F32),
+            pltpu.VMEM((SEQS, 1, LANES), F32),
+            pltpu.VMEM((SEQS, FEW, LANES), F32),
             pltpu.VMEM((SEQS, PROPS, COLS), F32),
             pltpu.VMEM((SEQS, PROPS, COLS), BF16),
-            pltpu.VMEM((NKV, PROPS, COLS + LANES), F32),
+            pltpu.VMEM((NKV, PROPS, COLS), F32),
+            pltpu.VMEM((NKV, 1, LANES), F32),
+            pltpu.VMEM((NKV, FEW, LANES), F32),
             pltpu.VMEM((NKV, PROPS, COLS), F32),
             pltpu.VMEM((NKV, PROPS, COLS), BF16),
             pltpu.VMEM((SEQS, PROPS, COLS), BF16),
-            pltpu.VMEM((SEQS, PROPS, COLS + LANES), BF16),
-            pltpu.VMEM((NKV, PROPS, COLS + LANES), BF16),
+            pltpu.VMEM((1, LANES), F32),
+            pltpu.VMEM((PROPS, LANES), F32),
+            pltpu.VMEM((SEQS, PROPS, COLS), BF16),
+            pltpu.VMEM((SEQS, FEW, LANES), F32),
+            pltpu.VMEM((NKV, PROPS, COLS), BF16),
+            pltpu.VMEM((NKV, FEW, LANES), F32),
             pltpu.VMEM((PROPS, COLS), BF16),
             pltpu.VMEM((2, HALF, COLS), BF16),
             pltpu.VMEM((NTP, PROPS, COLS), BF16),
@@ -666,8 +699,14 @@
             dma((NKV,)),
             dma((SEQS,)),
             dma((NKV,)),
+            dma((SEQS,)),
             dma((NKV,)),
             dma((SEQS,)),
+            dma((NKV,)),
+            dma((NKV,)),
+            dma((SEQS,)),
+            dma((SEQS,)),
+            dma((NKV,)),
             dma((SEQS,)),
             dma((NKV,)),
             dma((2 * NKV,)),

time: 42.2 us -> 41 us (0.972)
  Pallas kernels: 40.7 us -> 39.5 us
    pallas_call x1, Pallas kernels: 40.7 us -> 39.5 us  [body(): pl.pallas_call(kernel, out_shape=jax.ShapeDtypeStruct((OUT_ROWS, COLS), B...]
where the time goes in v4:
time: 41 us; the launch traced here: 40.8 us
  Pallas kernels  39.5 us (96%)
  local copies, waits for them, and re-layouts  1.34 us (3%)
    pallas_call x1, Pallas kernels, body(): pl.pallas_call(kernel, out_shape=jax.ShapeDtypeStruct((OUT_ROWS, COLS), B...  39.5 us
    unnamed x1, local copies, waits for them, and re-layouts  1.34 us

profile of v4, /device:TPU:1, one launch (start us, length us, event | category | flops | bytes accessed | tf_op | source)
XLA Modules:
  0.0 40.8 jit_solution(7134188436261993586)
XLA Ops:
  0.0 39.5 %tree_attention.1 = bf16[36,256]{1,0:T(8,128)(2,1)} custom-call(bf16[288,256]{1,0:T(8,128)(2,1)} %tokens.1, f32[1,256]{1,0:T(1,128)} %bitcast.3, bf16[256,256]{1,0:T(8,128)(2,1)} %wq.1, bf16[256,256]{1,0:T(8,128)(2,1)} %wk.1, bf16[256,256]{1,0:T(8,128)(2,1)} %wv.1, bf16[32,4096]{1,0:T(8,128)(2,1)} %bitcast.2, f32[32]{0:T(128)} %bias.1, bf16[256,256]{1,0:T(8,128)(2,1)} %wo.1, ...), custom_call_target="tpu_custom_call" | custom-call | tf_op jit(solution)/shard_map/tree_attention/pallas_call | solution.py:655
  39.5 1.3 %copy.15 = bf16[36,256]{1,0:T(8,128)(2,1)} copy(bf16[36,256]{1,0:T(8,128)(2,1)} %tree_attention.1) | data formatting | bytes 36864

commit v5 on v4

--- a/solution.py
+++ b/solution.py
@@ -26,6 +26,7 @@
 GROUP = 3
 HALF = 16
 FEW = 8
+IN_ORDER = (0, 1, 4, 3, 2, 5, 8, 7, 6, 9, 12, 11, 10, 13, 15, 14)
 FAR_FIRST = sorted(
     [(z, x) for z in range(4) for x in range(4) if z or x],
     key=lambda d: -sum(min(n, 4 - n) for n in d),
@@ -116,12 +117,10 @@
     v_par,
     s_q,
     s_sq,
-    s_x,
     s_k,
     s_v,
     r_q,
     r_sq,
-    r_x,
     r_k,
     r_v,
     g_q,
@@ -140,8 +139,6 @@
     q_recv,
     z_send,
     z_recv,
-    x_send,
-    x_recv,
     k_send,
     k_recv,
     v_send,
@@ -285,25 +282,23 @@
         for r in range(1, NKV):
             gather_copy(buf, send, recv, below(kv + r, NKV), r, mine).wait_send()
 
-    def whole_copy(distance):
-        z, x = at_distance(*distance)
+    def whole_copy(to):
         return pltpu.make_async_remote_copy(
             src_ref=s_att,
             dst_ref=r_att.at[tp],
-            send_sem=a_send.at[4 * distance[0] + distance[1]],
+            send_sem=a_send.at[to],
             recv_sem=a_recv.at[tp],
-            device_id={"kv": 4 * z + x, "tp": whole_to},
+            device_id={"kv": to, "tp": whole_to},
             device_id_type=MESH,
         )
 
-    def half_copy(distance, c):
-        z, x = at_distance(*distance)
+    def half_copy(to, c):
         return pltpu.make_async_remote_copy(
             src_ref=s_half.at[c],
             dst_ref=r_half.at[tp],
-            send_sem=a_send.at[NKV * c + 4 * distance[0] + distance[1]],
+            send_sem=a_send.at[NKV * c + to],
             recv_sem=a_recv.at[NTP + tp],
-            device_id={"kv": 4 * z + x, "tp": 2 * out_group + c},
+            device_id={"kv": to, "tp": 2 * out_group + c},
             device_id_type=MESH,
         )
 
@@ -338,11 +333,17 @@
         square_rows[:FEW],
     )
     rows = jnp.concatenate([rows, jnp.zeros((FEW, 3 * LANES - ROWS), F32)], axis=1)
+    wide_row = lax.broadcasted_iota(jnp.int32, rows.shape, 0)
+    placed = rows
+    for h in range(1, HEADS + 1):
+        placed = jnp.where(wide_row == h, pltpu.roll(rows, h * PROPS, 1), placed)
+    few_row = lax.broadcasted_iota(jnp.int32, (FEW, LANES), 0)
+    few_lane = lax.broadcasted_iota(jnp.int32, (FEW, LANES), 1) - PROPS * few_row
+    kept = (few_lane >= 0) & (few_lane < PROPS) & (few_row <= HEADS)
     for seq in range(SEQS):
         shift = (3 * LANES - seq * PROPS) % (3 * LANES)
-        turned = pltpu.roll(rows, shift, 1) if shift else rows
-        s_x[seq] = turned[:, :LANES]
-        s_sq[seq] = turned[HEADS : HEADS + 1, :LANES]
+        turned = pltpu.roll(placed, shift, 1) if shift else placed
+        s_sq[seq] = jnp.sum(jnp.where(kept, turned[:, :LANES], 0.0), axis=0, keepdims=True)
 
     pl.semaphore_wait(barrier, greeted)
     to_owners(s_sq, r_sq, z_send, z_recv)
@@ -391,9 +392,10 @@
         summed = r_sq[0]
         for i in range(1, NKV):
             summed = summed + r_sq[i]
-        i_row[...] = lax.rsqrt(summed / FULL_WIDTH + 1e-6)
-        on_diagonal = lane == lax.broadcasted_iota(jnp.int32, (PROPS, LANES), 0)
-        inverse = jnp.sum(jnp.where(on_diagonal, i_row[...], 0.0), axis=1, keepdims=True)
+        i_row[...] = summed
+        on_diagonal = lane == HEADS * PROPS + lax.broadcasted_iota(jnp.int32, (PROPS, LANES), 0)
+        own_squares = jnp.sum(jnp.where(on_diagonal, summed, 0.0), axis=1, keepdims=True)
+        inverse = lax.rsqrt(own_squares / FULL_WIDTH + 1e-6)
         i_col[...] = jnp.broadcast_to(inverse, (PROPS, LANES))
         arrived(s_q, r_q, q_send, q_recv)
         total = r_q[0]
@@ -403,8 +405,6 @@
         to_all(g_q, gq_send, gq_recv)
 
     pending.append(lambda: pl.when(is_owner)(lambda: sent_to_all(g_q, gq_send, gq_recv)))
-    to_owners(s_x, r_x, x_send, x_recv)
-    pending.append(lambda: sent_to_owners(s_x, r_x, x_send, x_recv))
     to_owners(s_k, r_k, k_send, k_recv)
     pending.append(lambda: sent_to_owners(s_k, r_k, k_send, k_recv))
     to_owners(s_v, r_v, v_send, v_recv)
@@ -418,14 +418,15 @@
     l_cv.wait()
     position = kv * POS + lax.broadcasted_iota(jnp.int32, (1, POS), 1)
 
-    def stat_rows(top, total):
-        stats = jnp.zeros((PROPS, LANES), F32)
+    own_lane = wide - lax.broadcasted_iota(jnp.int32, (PROPS, COLS), 0)
+
+    def stat_row(top, total):
+        stats = jnp.zeros((PROPS, COLS), F32)
         for h in range(HEADS):
             own = slice(h * PROPS, (h + 1) * PROPS)
-            stats = jnp.where(lane == h, top[own], stats)
-            stats = jnp.where(lane == HEADS + h, total[own], stats)
-        padded = jnp.concatenate([stats, jnp.zeros((LANES - PROPS, LANES), F32)], axis=0)
-        return padded.T[:FEW]
+            stats = jnp.where(own_lane == h * PROPS, top[own], stats)
+            stats = jnp.where(own_lane == (HEADS + h) * PROPS, total[own], stats)
+        return jnp.sum(stats, axis=0, keepdims=True)
 
     def attend(seq):
         q = by_head(g_q[seq].astype(F32) * (HEAD_DIM**-0.5), wide).astype(BF16)
@@ -441,7 +442,7 @@
         total = jnp.sum(weights, axis=1, keepdims=True)
         mix = jnp.dot(weights.astype(BF16), v_cv[seq], preferred_element_type=F32)
         s_mix[seq] = diagonal(mix, lane).astype(BF16)
-        s_stat[seq] = stat_rows(top, total)
+        s_stat[seq] = stat_row(top, total)
 
     def attend_group(j, carry):
         seqs = [seq_at(below(index + SEQS - j * GROUP - u, SEQS)) for u in range(GROUP)]
@@ -468,17 +469,17 @@
         r_v[kv] = s_v[mine]
         r_mix[kv] = s_mix[mine]
         r_stat[kv] = s_stat[mine]
-        r_x[kv] = s_x[mine]
         inverse = i_col[:, 0:1]
         head_row = lax.broadcasted_iota(jnp.int32, (FEW, LANES), 0)
         shift = jnp.zeros((FEW, LANES), F32)
         for h in range(HEADS):
             shift = jnp.where(head_row == h, v_bias[tp * HEADS + h], shift)
-        arrived(s_x, r_x, x_send, x_recv)
-        gates = r_x[0]
-        for i in range(1, NKV):
-            gates = gates + r_x[i]
-        gates = i_row[...] * gates + shift
+        summed = jnp.broadcast_to(i_row[...], (FEW, LANES))
+        gates = summed
+        for h in range(1, HEADS):
+            gates = jnp.where(head_row == h, pltpu.roll(summed, LANES - h * PROPS, 1), gates)
+        own_squares = pltpu.roll(summed, LANES - HEADS * PROPS, 1)
+        gates = lax.rsqrt(own_squares / FULL_WIDTH + 1e-6) * gates + shift
         log_gates = jnp.minimum(gates, 0.0) - jnp.log1p(jnp.exp(-jnp.abs(gates)))
         square = (PROPS, PROPS)
         older = lax.broadcasted_iota(jnp.int32, square, 0)
@@ -517,36 +518,44 @@
         tree_mix = diagonal(
             jnp.dot(weights.astype(BF16), new_values, preferred_element_type=F32), lane
         )
-        tree_stats = stat_rows(tree_top, tree_total)
+        tree_stats = stat_row(tree_top, tree_total)
 
         arrived(s_stat, r_stat, y_send, y_recv)
         stats = [r_stat[i] for i in range(NKV)] + [tree_stats]
         best = functools.reduce(jnp.maximum, stats)
         factors = [jnp.exp(s - best) for s in stats]
         denominator = functools.reduce(
-            jnp.add, [pltpu.roll(s, HEADS, 0) * f for s, f in zip(stats, factors)]
+            jnp.add,
+            [pltpu.roll(s, COLS - HEADS * PROPS, 1) * f for s, f in zip(stats, factors)],
         )
         under = 1.0 / denominator
-        columns = jnp.concatenate([f * under for f in factors[:NKV]], axis=0).T[:PROPS]
-        tree_columns = jnp.concatenate(
-            [factors[NKV] * under, jnp.zeros((LANES - FEW, LANES), F32)], axis=0
-        ).T[:PROPS]
-        attended = tree_mix * spread([tree_columns[:, h : h + 1] for h in range(HEADS)], lane)
+        shares = jnp.concatenate(
+            [(f * under)[:, :LANES] for f in factors]
+            + [jnp.zeros((LANES - NKV - 1, LANES), F32)],
+            axis=0,
+        )
+        used = lax.broadcasted_iota(jnp.int32, shares.shape, 1) < HEADS * PROPS
+        shares = jnp.where(used, shares, 0.0).T
+
+        def share_of(i):
+            return spread(
+                [shares[h * PROPS : (h + 1) * PROPS, i : i + 1] for h in range(HEADS)], lane
+            )
+
+        attended = tree_mix * share_of(NKV)
         arrived(s_mix, r_mix, m_send, m_recv)
         for i in range(NKV):
-            shares = [columns[:, FEW * i + h : FEW * i + h + 1] for h in range(HEADS)]
-            attended = attended + r_mix[i].astype(F32) * spread(shares, lane)
+            attended = attended + r_mix[i].astype(F32) * share_of(i)
 
         @pl.when(out_place != 1)
         def _():
             s_att[...] = attended.astype(BF16)
 
-            for distance in FAR_FIRST:
-                whole_copy(distance).start()
-
-            @pl.when(tp != whole_to)
-            def _():
-                whole_copy((0, 0)).start()
+            for to in IN_ORDER:
+
+                @pl.when((kv != to) | (tp != whole_to))
+                def _():
+                    whole_copy(to).start()
 
             @pl.when(tp == whole_to)
             def _():
@@ -557,38 +566,31 @@
             s_half[0] = attended[:HALF].astype(BF16)
             s_half[1] = attended[PROPS - HALF :].astype(BF16)
 
-            for distance in FAR_FIRST:
-                half_copy(distance, 0).start()
-                half_copy(distance, 1).start()
+            for to in IN_ORDER:
+                for c in range(2):
+
+                    @pl.when((kv != to) | (tp != 2 * out_group + c))
+                    def _():
+                        half_copy(to, c).start()
+
             for c in range(2):
-
-                @pl.when(tp != 2 * out_group + c)
-                def _():
-                    half_copy((0, 0), c).start()
 
                 @pl.when(tp == 2 * out_group + c)
                 def _():
                     r_half[tp] = s_half[c]
 
     def scattered():
-        @pl.when(is_whole)
-        def _():
-            for distance in FAR_FIRST:
-                whole_copy(distance).wait_send()
-
-            @pl.when(tp != whole_to)
+        for to in IN_ORDER:
+
+            @pl.when(is_whole & ((kv != to) | (tp != whole_to)))
             def _():
-                whole_copy((0, 0)).wait_send()
-
-        @pl.when(is_half)
-        def _():
+                whole_copy(to).wait_send()
+
             for c in range(2):
-                for distance in FAR_FIRST:
-                    half_copy(distance, c).wait_send()
-
-                @pl.when(tp != 2 * out_group + c)
+
+                @pl.when(is_half & ((kv != to) | (tp != 2 * out_group + c)))
                 def _():
-                    half_copy((0, 0), c).wait_send()
+                    half_copy(to, c).wait_send()
 
     lax.fori_loop(1, NTP, weight_arrived, 0)
     for wait in pending:
@@ -673,28 +675,24 @@
             pltpu.VMEM((SEQS, PROPS), jnp.int32),
             pltpu.VMEM((SEQS, PROPS, COLS), F32),
             pltpu.VMEM((SEQS, 1, LANES), F32),
-            pltpu.VMEM((SEQS, FEW, LANES), F32),
             pltpu.VMEM((SEQS, PROPS, COLS), F32),
             pltpu.VMEM((SEQS, PROPS, COLS), BF16),
             pltpu.VMEM((NKV, PROPS, COLS), F32),
             pltpu.VMEM((NKV, 1, LANES), F32),
-            pltpu.VMEM((NKV, FEW, LANES), F32),
             pltpu.VMEM((NKV, PROPS, COLS), F32),
             pltpu.VMEM((NKV, PROPS, COLS), BF16),
             pltpu.VMEM((SEQS, PROPS, COLS), BF16),
             pltpu.VMEM((1, LANES), F32),
             pltpu.VMEM((PROPS, LANES), F32),
             pltpu.VMEM((SEQS, PROPS, COLS), BF16),
-            pltpu.VMEM((SEQS, FEW, LANES), F32),
+            pltpu.VMEM((SEQS, 1, COLS), F32),
             pltpu.VMEM((NKV, PROPS, COLS), BF16),
-            pltpu.VMEM((NKV, FEW, LANES), F32),
+            pltpu.VMEM((NKV, 1, COLS), F32),
             pltpu.VMEM((PROPS, COLS), BF16),
             pltpu.VMEM((2, HALF, COLS), BF16),
             pltpu.VMEM((NTP, PROPS, COLS), BF16),
             pltpu.VMEM((NTP, HALF, COLS), BF16),
             dma((13,)),
-            dma((SEQS,)),
-            dma((NKV,)),
             dma((SEQS,)),
             dma((NKV,)),
             dma((SEQS,)),

time: 41 us -> 40 us (0.976)
  Pallas kernels: 39.5 us -> 38.5 us
    pallas_call x1, Pallas kernels: 39.5 us -> 38.5 us  [body(): pl.pallas_call(kernel, out_shape=jax.ShapeDtypeStruct((OUT_ROWS, COLS), B...]
where the time goes in v5:
time: 40 us; the launch traced here: 39.8 us
  Pallas kernels  38.5 us (96%)
  local copies, waits for them, and re-layouts  1.34 us (3%)
    pallas_call x1, Pallas kernels, body(): pl.pallas_call(kernel, out_shape=jax.ShapeDtypeStruct((OUT_ROWS, COLS), B...  38.5 us
    unnamed x1, local copies, waits for them, and re-layouts  1.34 us

profile of v5, /device:TPU:1, one launch (start us, length us, event | category | flops | bytes accessed | tf_op | source)
XLA Modules:
  0.0 39.8 jit_solution(7922196110259031259)
XLA Ops:
  0.0 38.5 %tree_attention.1 = bf16[36,256]{1,0:T(8,128)(2,1)} custom-call(bf16[288,256]{1,0:T(8,128)(2,1)} %tokens.1, f32[1,256]{1,0:T(1,128)} %bitcast.3, bf16[256,256]{1,0:T(8,128)(2,1)} %wq.1, bf16[256,256]{1,0:T(8,128)(2,1)} %wk.1, bf16[256,256]{1,0:T(8,128)(2,1)} %wv.1, bf16[32,4096]{1,0:T(8,128)(2,1)} %bitcast.2, f32[32]{0:T(128)} %bias.1, bf16[256,256]{1,0:T(8,128)(2,1)} %wo.1, ...), custom_call_target="tpu_custom_call" | custom-call | tf_op jit(solution)/shard_map/tree_attention/pallas_call | solution.py:657
  38.5 1.3 %copy.15 = bf16[36,256]{1,0:T(8,128)(2,1)} copy(bf16[36,256]{1,0:T(8,128)(2,1)} %tree_attention.1) | data formatting | bytes 36864

commit v6 on v5

--- a/solution.py
+++ b/solution.py
@@ -194,10 +194,9 @@
     l_tok, l_gain, l_wq, l_gw, l_wk, l_wv, l_ck, l_cd, l_cv, l_wo, l_len, l_bias, l_par = loads
 
     barrier = pltpu.get_barrier_semaphore()
-    for r in range(1, NKV):
-        pl.semaphore_signal(
-            barrier, inc=1, device_id={"kv": below(kv + r, NKV)}, device_id_type=MESH
-        )
+    for distance in FAR_FIRST:
+        to = 4 * below(row + distance[0], 4) + below(column + distance[1], 4)
+        pl.semaphore_signal(barrier, inc=1, device_id={"kv": to}, device_id_type=MESH)
     for r in range(1, NTP):
         pl.semaphore_signal(
             barrier, inc=1, device_id={"tp": below(tp + r, NTP)}, device_id_type=MESH
@@ -580,6 +579,11 @@
                     r_half[tp] = s_half[c]
 
     def scattered():
+        @pl.when(is_owner)
+        def _():
+            sent_in_order()
+
+    def sent_in_order():
         for to in IN_ORDER:
 
             @pl.when(is_whole & ((kv != to) | (tp != whole_to)))

time: 40 us -> 39.8 us (level)
  no operation moved by 1% of the time
where the time goes in v6:
time: 39.8 us; the launch traced here: 39.6 us
  Pallas kernels  38.3 us (96%)
  local copies, waits for them, and re-layouts  1.34 us (3%)
    pallas_call x1, Pallas kernels, body(): pl.pallas_call(kernel, out_shape=jax.ShapeDtypeStruct((OUT_ROWS, COLS), B...  38.3 us
    unnamed x1, local copies, waits for them, and re-layouts  1.34 us

profile of v6, /device:TPU:1, one launch (start us, length us, event | category | flops | bytes accessed | tf_op | source)
XLA Modules:
  0.0 39.6 jit_solution(15808389931586541564)
XLA Ops:
  0.0 38.3 %tree_attention.1 = bf16[36,256]{1,0:T(8,128)(2,1)} custom-call(bf16[288,256]{1,0:T(8,128)(2,1)} %tokens.1, f32[1,256]{1,0:T(1,128)} %bitcast.3, bf16[256,256]{1,0:T(8,128)(2,1)} %wq.1, bf16[256,256]{1,0:T(8,128)(2,1)} %wk.1, bf16[256,256]{1,0:T(8,128)(2,1)} %wv.1, bf16[32,4096]{1,0:T(8,128)(2,1)} %bitcast.2, f32[32]{0:T(128)} %bias.1, bf16[256,256]{1,0:T(8,128)(2,1)} %wo.1, ...), custom_call_target="tpu_custom_call" | custom-call | tf_op jit(solution)/shard_map/tree_attention/pallas_call | solution.py:661
  38.3 1.3 %copy.15 = bf16[36,256]{1,0:T(8,128)(2,1)} copy(bf16[36,256]{1,0:T(8,128)(2,1)} %tree_attention.1) | data formatting | bytes 36864
